TPU v7x, 32 devices: a whole 2x2x4 slice. The times are simulated.
32 devices in a mesh: sp: 8 (over z, x), tp: 4 (over y, core).
Axes of the slice: x: 2, y: 2, z: 4, core: 2. Of those that a mesh axis runs over, the one named last changes fastest.
Arguments:
- cotangent: bfloat16 [2048, 2048], P('sp', 'tp'), may hold values from -6 to 6
- moe_input: bfloat16 [2048, 2048], P('sp', 'tp'), may hold values from -6 to 6
- routes: int32 [2048, 2], P('sp'), may hold values from 0 to 7, all different within a row; in each aligned block of 256 rows (0 to 255, 256 to 511, ...) at most 96 rows name the same one
- gates: float32 [2048, 2], P('sp'), may hold values from 0.1 to 1
- w_gate: bfloat16 [8, 2048, 2048], P('sp', None, 'tp'), may hold values from -0.125 to 0.125
- w_up: bfloat16 [8, 2048, 2048], P('sp', None, 'tp'), may hold values from -0.125 to 0.125
- w_down: bfloat16 [8, 2048, 2048], P('sp', 'tp'), may hold values from -0.125 to 0.125
- out_proj: bfloat16 [1024, 2048], P('tp'), may hold values from -0.1875 to 0.1875
- conv_in: bfloat16 [1024, 2048], P('tp', 'sp'), may hold values from -6 to 6
- branch: bfloat16 [1024, 2048], P('tp', 'sp'), may hold values from -6 to 6
- state_before: float32 [1024, 2048], P('tp', 'sp'), may hold values from -6 to 6
- state_after: float32 [1024, 2048], P('tp', 'sp'), may hold values from -6 to 6
- jump: float32 [1024, 2048], P('tp', 'sp'), may hold values from -2 to 0, as said below
- recur_weight: bfloat16 [2, 16, 64, 64], P(None, 'tp'), may hold values from -0.75 to 0.75
- input_weight: bfloat16 [2, 16, 64, 64], P(None, 'tp'), may hold values from -0.75 to 0.75
- lam: float32 [2, 1024], P(None, 'tp')
Outputs:
- gate_grad: bfloat16 [8, 2048, 2048], P('sp', None, 'tp')
- up_grad: bfloat16 [8, 2048, 2048], P('sp', None, 'tp')
- down_grad: bfloat16 [8, 2048, 2048], P('sp', 'tp')
- residual_grad: bfloat16 [2048, 2048], P('sp', 'tp')
- out_proj_grad: float32 [1024, 2048], P('tp', 'sp')
- conv_grad: float32 [1024, 2048], P('tp', 'sp')
- branch_grad: float32 [1024, 2048], P('tp', 'sp')
Inputs may be any that keep to these rules, and one draw needn't show every extreme that they name: `routes`: each token names 2 different experts. Among the tokens of one index of sp (aligned blocks of 256 rows) no expert is named more than 96 times, a bound that some block reaches. `jump`: every entry is at most -1 / 20480.
All inputs are finite; a program needn't handle non-finite values.
Results may differ from a plain program's by a relative error of at most 0.02.
Values may be sent and summed in bfloat16 or wider, within the bound.
A program may use at most 128 MiB of HBM per device.

v0:
```python
import jax
import jax.numpy as jnp
from jax import lax
from jax.experimental import pallas as pl
from jax.experimental.pallas import tpu as pltpu
from jax.sharding import PartitionSpec as P

decay_scale = 8.0


MESH = pl.DeviceIdType.MESH
VMEM_SPEC = pl.BlockSpec(memory_space=pltpu.VMEM)


def at(sp=None, tp=None):
    sp = lax.axis_index("sp") if sp is None else sp
    tp = lax.axis_index("tp") if tp is None else tp
    return (sp, tp)


def meet(devices):
    barrier = pltpu.get_barrier_semaphore()
    for device in devices:
        pl.semaphore_signal(barrier, inc=1, device_id=device, device_id_type=MESH)
    pl.semaphore_wait(barrier, len(devices))


def remote(source, target, send, recv, device):
    return pltpu.make_async_remote_copy(
        src_ref=source, dst_ref=target, send_sem=send, recv_sem=recv,
        device_id=device, device_id_type=MESH,
    )


def params(collective_id):
    return pltpu.CompilerParams(
        collective_id=collective_id, has_side_effects=True, vmem_limit_bytes=48 * 1024 * 1024
    )


def dispatch(send_rows, send_grads):
    n, tp = lax.axis_size("sp"), lax.axis_size("tp")
    chips = tp // 2
    capacity, width = send_rows.shape[1:]
    groups = min(n, 8)
    span = n // groups

    def kernel(rows_ref, grads_ref, rows_out, grads_out, ss, sr, ps, pr, ys, yr, fs, fr):
        me, place = lax.axis_index("sp"), lax.axis_index("tp")
        chip, core = place // 2, place % 2
        partner = chip * 2 + (1 - core)
        group, inner = me // span, me % span
        pairs = ((rows_ref, rows_out), (grads_ref, grads_out))

        def columns(member):
            return pl.ds(pl.multiple_of(member * width, width), width)

        def peer(step, sign):
            other_group = lax.rem(group + sign * (step // span) + groups, groups)
            return other_group * span + lax.rem(inner + sign * (step % span) + span, span)

        def across(turn, sign):
            return lax.rem(chip + sign * turn + chips, chips) * 2 + core

        meet(
            [at(sp=peer(k, 1)) for k in range(1, n)]
            + [at(tp=partner)]
            + [at(tp=across(t, 1)) for t in range(1, chips)]
        )
        mine = columns(place)
        first = []
        for k in range(1, n):
            to = peer(k, 1)
            for kind, (source, out) in enumerate(pairs):
                copy = remote(
                    source.at[to], out.at[me, :, mine],
                    ss.at[k, kind], sr.at[k, kind], at(sp=to),
                )
                copy.start()
                first.append(copy)
        for source, out in pairs:
            out[me, :, mine] = source[me]
        sent = []
        for g in range(groups):
            base = lax.rem(group - g + groups, groups) * span
            for kind, (source, out) in enumerate(pairs):
                for i in range(span):
                    k = g * span + i
                    if k == 0:
                        continue
                    origin = peer(k, -1)
                    remote(
                        source.at[origin], out.at[origin, :, mine],
                        ss.at[k, kind], sr.at[k, kind], at(sp=origin),
                    ).wait_recv()
                block = out.at[pl.ds(base, span), :, mine]
                if g == 0 and span == 1:
                    block = source.at[pl.ds(base, span)]
                landing = out.at[pl.ds(base, span), :, mine]
                for t in range(1, chips):
                    copy = remote(
                        block, landing, ys.at[g, t, kind], yr.at[g, t, kind], at(tp=across(t, 1))
                    )
                    copy.start()
                    sent.append(copy)
                copy = remote(block, landing, ps.at[g, kind], pr.at[g, kind], at(tp=partner))
                copy.start()
                sent.append(copy)
        for g in range(groups):
            base = lax.rem(group - g + groups, groups) * span
            for kind, (source, out) in enumerate(pairs):
                for t in range(1, chips):
                    block = out.at[pl.ds(base, span), :, columns(across(t, -1))]
                    remote(
                        block, block, ys.at[g, t, kind], yr.at[g, t, kind], at(tp=across(t, -1))
                    ).wait_recv()
                    copy = remote(
                        block, block, fs.at[g, t, kind], fr.at[g, t, kind], at(tp=partner)
                    )
                    copy.start()
                    sent.append(copy)
        for g in range(groups):
            base = lax.rem(group - g + groups, groups) * span
            for kind, (source, out) in enumerate(pairs):
                block = out.at[pl.ds(base, span), :, columns(partner)]
                remote(block, block, ps.at[g, kind], pr.at[g, kind], at(tp=partner)).wait_recv()
                for t in range(1, chips):
                    member = lax.rem(chip - t + chips, chips) * 2 + (1 - core)
                    block = out.at[pl.ds(base, span), :, columns(member)]
                    remote(
                        block, block, fs.at[g, t, kind], fr.at[g, t, kind], at(tp=partner)
                    ).wait_recv()
        for copy in first + sent:
            copy.wait_send()

    full = jax.ShapeDtypeStruct((n, capacity, tp * width), send_rows.dtype)
    dma = pltpu.SemaphoreType.DMA
    sems = [dma((n, 2))] * 2 + [dma((groups, 2))] * 2 + [dma((groups, max(chips, 2), 2))] * 4
    return pl.pallas_call(
        kernel, name="dispatch", out_shape=(full, full),
        in_specs=[VMEM_SPEC] * 2, out_specs=(VMEM_SPEC,) * 2,
        scratch_shapes=sems, compiler_params=params(1),
    )(send_rows, send_grads)


def scatter_sum(partial):
    tp = lax.axis_size("tp")
    chips = tp // 2
    rows, full = partial.shape
    width = full // tp
    strip = 32

    def kernel(part_ref, out_ref, near, total, far, own, ns, nr, ys, yr):
        place = lax.axis_index("tp")
        chip, core = place // 2, place % 2
        partner = chip * 2 + (1 - core)

        def columns(member):
            return pl.ds(pl.multiple_of(member * width, width), width)

        def turned(t, sign):
            return lax.rem(chip + sign * t + chips, chips)

        meet([at(tp=partner)] + [at(tp=turned(t, 1) * 2 + core) for t in range(1, chips)])
        order = list(range(1, chips)) + [0]
        copies = []
        for t in order:
            copy = remote(
                part_ref.at[:, columns(turned(t, 1) * 2 + (1 - core))],
                near.at[t], ns.at[t], nr.at[t], at(tp=partner),
            )
            copy.start()
            copies.append(copy)
        for t, copy in zip(order, copies):
            copy.wait_recv()
            mine = columns(turned(t, 1) * 2 + core)

            @pl.loop(0, rows // strip)
            def _(i):
                where = pl.ds(pl.multiple_of(i * strip, strip), strip)
                value = part_ref[where, mine].astype(jnp.float32) + near[t, where].astype(
                    jnp.float32
                )
                if t == 0:
                    own[where] = value
                else:
                    total[t, where] = value.astype(total.dtype)

        sends = []
        for t in range(1, chips):
            copy = remote(
                total.at[t], far.at[t], ys.at[t], yr.at[t], at(tp=turned(t, 1) * 2 + core)
            )
            copy.start()
            sends.append(copy)
        for copy in sends:
            copy.wait_recv()

        @pl.loop(0, rows // strip)
        def _(i):
            where = pl.ds(pl.multiple_of(i * strip, strip), strip)
            value = own[where]
            for t in range(1, chips):
                value = value + far[t, where].astype(jnp.float32)
            out_ref[where] = value.astype(out_ref.dtype)

        for copy in copies + sends:
            copy.wait_send()

    dma = pltpu.SemaphoreType.DMA
    block = pltpu.VMEM((chips, rows, width), partial.dtype)
    return pl.pallas_call(
        kernel, name="scatter_sum",
        out_shape=jax.ShapeDtypeStruct((rows, width), partial.dtype),
        in_specs=[VMEM_SPEC], out_specs=VMEM_SPEC,
        scratch_shapes=[block, block, block, pltpu.VMEM((rows, width), jnp.float32)]
        + [dma((chips,))] * 4,
        compiler_params=params(2),
    )(partial)


def share(values):
    n = lax.axis_size("sp")

    def kernel(in_ref, out_ref, ss, sr):
        me = lax.axis_index("sp")
        meet([at(sp=lax.rem(me + k, n)) for k in range(1, n)])
        copies = []
        for k in range(1, n):
            copy = remote(
                in_ref, out_ref.at[me], ss.at[k], sr.at[k], at(sp=lax.rem(me + k, n))
            )
            copy.start()
            copies.append(copy)
        out_ref[me] = in_ref[...]
        for k in range(1, n):
            origin = lax.rem(me - k + n, n)
            remote(in_ref, out_ref.at[origin], ss.at[k], sr.at[k], at(sp=origin)).wait_recv()
        for copy in copies:
            copy.wait_send()

    dma = pltpu.SemaphoreType.DMA
    return pl.pallas_call(
        kernel, name="share",
        out_shape=jax.ShapeDtypeStruct((n,) + values.shape, values.dtype),
        in_specs=[VMEM_SPEC], out_specs=VMEM_SPEC,
        scratch_shapes=[dma((n,))] * 2, compiler_params=params(3),
    )(values)


def silu_parts(pre_act):
    sigmoid_val = jax.nn.sigmoid(pre_act)
    return (pre_act * sigmoid_val, sigmoid_val * (1.0 + pre_act * (1.0 - sigmoid_val)))


def block_map(values, weight):
    return jnp.einsum("nit,nij->njt", values, weight, preferred_element_type=jnp.float32)


def block_back(gradient, weight):
    return jnp.einsum(
        "njt,nij->nit", gradient, weight.astype(jnp.float32), precision=lax.Precision.HIGHEST
    )


def gate_values(conv_in, weight_r, weight_i, lam_row, jump):
    channels, length = conv_in.shape
    shaped = conv_in.reshape(weight_r.shape[0], weight_r.shape[1], length)
    recur_gate = jax.nn.sigmoid(block_map(shaped, weight_r).reshape(channels, length))
    inward = jax.nn.sigmoid(block_map(shaped, weight_i).reshape(channels, length))
    speed_row = decay_scale * jax.nn.softplus(-lam_row)[:, None]
    log_decay = -speed_row * recur_gate + jump
    retain = jnp.exp(log_decay)
    root_term = jnp.sqrt(-jnp.expm1(2.0 * log_decay))
    conv_wide = conv_in.astype(jnp.float32)
    return (recur_gate, inward, speed_row, retain, root_term, conv_wide)


def gate_backward(pieces, decay_grad, drive_grad, weight_r, weight_i):
    recur_gate, inward, speed_row, retain, root_term, conv_wide = pieces
    channels, length = conv_wide.shape
    shape_three = (weight_r.shape[0], weight_r.shape[1], length)
    log_grad = decay_grad * retain - drive_grad * inward * conv_wide * retain * retain / root_term
    recur_grad = log_grad * -speed_row * recur_gate * (1.0 - recur_gate)
    inward_grad = drive_grad * root_term * conv_wide * inward * (1.0 - inward)
    direct = drive_grad * root_term * inward
    back_r = block_back(recur_grad.reshape(shape_three), weight_r)
    back_i = block_back(inward_grad.reshape(shape_three), weight_i)
    return direct + (back_r + back_i).reshape(channels, length)


def combine_pair(earlier, latter):
    return (earlier[0] * latter[0], latter[0] * earlier[1] + latter[1])


def expert_pass(full_rows, full_grads, gate_weight, up_weight, down_weight):
    contract_last = (((1,), (1,)), ((), ()))
    contract_first = (((0,), (0,)), ((), ()))
    pre_gate = jnp.dot(full_rows, gate_weight, preferred_element_type=jnp.float32)
    pre_up = jnp.dot(full_rows, up_weight, preferred_element_type=jnp.float32)
    silu_val, silu_slope = silu_parts(pre_gate)
    activation = (silu_val * pre_up).astype(jnp.bfloat16)
    act_grad = lax.dot_general(
        full_grads, down_weight, contract_last, preferred_element_type=jnp.float32
    )
    up_hidden = (act_grad * silu_val).astype(jnp.bfloat16)
    gate_hidden = (act_grad * pre_up * silu_slope).astype(jnp.bfloat16)
    partial_value = lax.dot_general(
        gate_hidden, gate_weight, contract_last, preferred_element_type=jnp.float32
    )
    partial_value = (
        partial_value
        + lax.dot_general(up_hidden, up_weight, contract_last, preferred_element_type=jnp.float32)
    ).astype(jnp.bfloat16)
    gate_acc = lax.dot_general(
        full_rows, gate_hidden, contract_first, preferred_element_type=jnp.float32
    )
    up_acc = lax.dot_general(
        full_rows, up_hidden, contract_first, preferred_element_type=jnp.float32
    )
    down_acc = lax.dot_general(
        activation, full_grads, contract_first, preferred_element_type=jnp.float32
    )
    return (partial_value, (gate_acc, up_acc, down_acc))


def on_device(
    cotangent,
    moe_input,
    routes,
    gates,
    w_gate,
    w_up,
    w_down,
    out_proj,
    conv_in,
    branch,
    state_before,
    state_after,
    jump,
    recur_weight,
    input_weight,
    lam,
):
    tokens_dev, width_dev = cotangent.shape
    per_token = routes.shape[1]
    experts = lax.axis_size("sp")
    capacity = 3 * tokens_dev // experts
    pair_total = tokens_dev * per_token
    routed = routes.reshape(-1)
    onehot = (routed[:, None] == jnp.arange(experts, dtype=jnp.int32)[None, :]).astype(jnp.int32)
    earlier_count = jnp.cumsum(onehot, axis=0) - onehot
    token_position = jnp.sum(earlier_count * onehot, axis=1)
    target = routed * capacity + token_position
    scaled = (cotangent.astype(jnp.float32)[:, None, :] * gates[:, :, None]).astype(jnp.bfloat16)
    scaled = scaled.reshape(pair_total, width_dev)
    copies = jnp.broadcast_to(moe_input[:, None, :], (tokens_dev, per_token, width_dev)).reshape(
        pair_total, width_dev
    )
    blank = jnp.zeros((experts * capacity, width_dev), jnp.bfloat16)
    send_rows = blank.at[target].set(copies).reshape(experts, capacity, width_dev)
    send_grads = blank.at[target].set(scaled).reshape(experts, capacity, width_dev)
    total_rows = experts * capacity
    full_rows, full_grads = dispatch(send_rows, send_grads)
    full_rows = full_rows.reshape(total_rows, -1)
    full_grads = full_grads.reshape(total_rows, -1)
    partial_value, totals = expert_pass(full_rows, full_grads, w_gate[0], w_up[0], w_down[0])
    row_grad = scatter_sum(partial_value)
    gate_grad = totals[0].astype(jnp.bfloat16)[None]
    up_grad = totals[1].astype(jnp.bfloat16)[None]
    down_grad = totals[2].astype(jnp.bfloat16)[None]
    returned = lax.all_to_all(
        row_grad.reshape(experts, capacity, width_dev),
        "sp",
        split_axis=0,
        concat_axis=0,
        tiled=True,
    )
    returned = returned.reshape(experts * capacity, width_dev)[target].reshape(
        tokens_dev, per_token, width_dev
    )
    residual_grad = (
        cotangent.astype(jnp.float32) + jnp.sum(returned.astype(jnp.float32), axis=1)
    ).astype(jnp.bfloat16)
    full_residual = lax.all_gather(residual_grad, "tp", axis=1, tiled=True)
    pieces_fwd = gate_values(conv_in, recur_weight[0], input_weight[0], lam[0], jump)
    pieces_bwd = gate_values(conv_in, recur_weight[1], input_weight[1], lam[1], jump)
    drive_fwd = pieces_fwd[4] * pieces_fwd[1] * pieces_fwd[5]
    drive_bwd = pieces_bwd[4] * pieces_bwd[1] * pieces_bwd[5]
    lru_out = pieces_fwd[3] * state_before + drive_fwd + pieces_bwd[3] * state_after + drive_bwd
    gelu_val, gelu_back = jax.vjp(jax.nn.gelu, branch.astype(jnp.float32))
    mix = (lru_out * gelu_val).astype(jnp.bfloat16)
    proj_part = lax.dot_general(
        full_residual, mix, (((0,), (1,)), ((), ())), preferred_element_type=jnp.float32
    ).astype(jnp.bfloat16)
    proj_part, full_residual = lax.optimization_barrier((proj_part, full_residual))
    proj_blocks = lax.all_to_all(
        proj_part.reshape(experts, -1, proj_part.shape[1]), "sp", split_axis=0, concat_axis=0, tiled=True
    )
    proj_rows = jnp.sum(proj_blocks.astype(jnp.float32), axis=0)
    out_proj_grad = proj_rows.T
    mix_grad = lax.dot_general(
        out_proj, full_residual, (((1,), (1,)), ((), ())), preferred_element_type=jnp.float32
    )
    lru_grad = mix_grad * gelu_val
    branch_grad = gelu_back(mix_grad * lru_out)[0]
    decay_fwd = pieces_fwd[3]
    decay_bwd = pieces_bwd[3]
    prod_fwd, local_fwd = lax.associative_scan(
        combine_pair, (decay_fwd, decay_fwd * lru_grad), reverse=True, axis=1
    )
    prod_bwd, local_bwd = lax.associative_scan(
        combine_pair, (decay_bwd, decay_bwd * lru_grad), axis=1
    )
    ends = jnp.concatenate([prod_fwd[:, 0], local_fwd[:, 0], prod_bwd[:, -1], local_bwd[:, -1]])
    shared = share(ends[None]).reshape(experts, 4, -1)
    place = lax.axis_index("sp")
    incoming_fwd = jnp.zeros_like(local_fwd[:, 0])
    incoming_bwd = jnp.zeros_like(incoming_fwd)
    for turn in range(experts - 1):
        late = experts - 1 - turn
        incoming_fwd = jnp.where(
            late > place, shared[late, 0] * incoming_fwd + shared[late, 1], incoming_fwd
        )
        incoming_bwd = jnp.where(
            turn < place, shared[turn, 2] * incoming_bwd + shared[turn, 3], incoming_bwd
        )
    carried_fwd = local_fwd + prod_fwd * incoming_fwd[:, None]
    carried_bwd = local_bwd + prod_bwd * incoming_bwd[:, None]
    delta_fwd = lru_grad + jnp.concatenate([carried_fwd[:, 1:], incoming_fwd[:, None]], axis=1)
    delta_bwd = lru_grad + jnp.concatenate([incoming_bwd[:, None], carried_bwd[:, :-1]], axis=1)
    conv_grad = gate_backward(
        pieces_fwd, delta_fwd * state_before, delta_fwd, recur_weight[0], input_weight[0]
    )
    conv_grad = conv_grad + gate_backward(
        pieces_bwd, delta_bwd * state_after, delta_bwd, recur_weight[1], input_weight[1]
    )
    return (gate_grad, up_grad, down_grad, residual_grad, out_proj_grad, conv_grad, branch_grad)


def solution(mesh):
    placed = (
        P("sp", "tp"),
        P("sp", "tp"),
        P("sp", None),
        P("sp", None),
        P("sp", None, "tp"),
        P("sp", None, "tp"),
        P("sp", "tp", None),
        P("tp", None),
        P("tp", "sp"),
        P("tp", "sp"),
        P("tp", "sp"),
        P("tp", "sp"),
        P("tp", "sp"),
        P(None, "tp", None, None),
        P(None, "tp", None, None),
        P(None, "tp"),
    )
    return jax.shard_map(
        on_device,
        mesh=mesh,
        in_specs=placed,
        out_specs=(
            P("sp", None, "tp"),
            P("sp", None, "tp"),
            P("sp", "tp", None),
            P("sp", "tp"),
            P("tp", "sp"),
            P("tp", "sp"),
            P("tp", "sp"),
        ),
        check_vma=False,
    )
```

profile of v0, /device:TPU:5, one launch (start us, length us, event | category | flops | bytes accessed | tf_op | source)
XLA Modules:
  0.0 257.8 jit_solution(13243403160919716500)
XLA Ops:
  9.4 1.1 reduce-window.6
  10.8 1.2 broadcast_in_dim.13
  12.1 1.0 reshape.587
  13.4 1.7 mul.648
  15.4 3.8 %scatter_custom_fusion = bf16[768,512]{1,0:T(8,128)(2,1)} fusion(s32[512]{0:T(512)S(1)} %bitcast.328, bf16[512,512]{1,0:T(8,128)(2,1)} %reshape.587, bf16[]{:T(256)} %constant.22.clone.1), kind=kCustom, calls=%fused_computation.63 | custom fusion | bytes 786944 | tf_op jit(solution)/shard_map/scatter | solution.py:361
  19.3 3.5 %scatter_custom_fusion.1 = bf16[768,512]{1,0:T(8,128)(2,1)S(1)} fusion(s32[512]{0:T(512)S(1)} %bitcast.329, f32[512,512]{1,0:T(8,128)} %mul.648, f32[512]{0:T(512)S(1)} %mul.649, bf16[]{:T(256)} %constant.22.clone.1), kind=kCustom, calls=%fused_computation.52 | custom fusion | flops 524288 | bytes 1837058 | tf_op jit(solution)/shard_map/scatter | solution.py:362
  22.8 1.1 copy-done.2
  23.9 52.0 %dispatch.1 = (bf16[8,96,2048]{2,1,0:T(8,128)(2,1)S(1)}, bf16[8,96,2048]{2,1,0:T(8,128)(2,1)}) custom-call(bf16[8,96,512]{2,1,0:T(8,128)(2,1)S(1)} %bitcast.305, bf16[8,96,512]{2,1,0:T(8,128)(2,1)S(1)} %bitcast.304), custom_call_target="tpu_custom_call" | custom-call | tf_op jit(solution)/shard_map/dispatch/pallas_call | solution.py:139
  76.0 1.8 fusion.5
  78.7 1.8 fusion.8
  81.2 1.2 copy-done.41
  82.4 2.3 multiply_convert_fusion.1
  84.7 1.8 fusion.3
  86.6 1.8 add_convert_fusion.part_ref
  88.4 24.0 %scatter_sum.1 = bf16[768,512]{1,0:T(8,128)(2,1)} custom-call(bf16[768,2048]{1,0:T(8,128)(2,1)S(1)} %add_convert_fusion.part_ref), custom_call_target="tpu_custom_call" | custom-call | tf_op jit(solution)/shard_map/scatter_sum/pallas_call | solution.py:212
  112.4 11.9 %all-to-all-start = ((bf16[8,96,512]{2,1,0:T(8,128)(2,1)}), bf16[8,96,512]{2,1,0:T(8,128)(2,1)S(1)}, u32[]{:S(2)}, u32[]{:S(2)}) async-start(bf16[8,96,512]{2,1,0:T(8,128)(2,1)} %bitcast.14), calls=%async_computation | async-start | bytes 1572864 | tf_op jit(solution)/shard_map/all_to_all | solution.py:372
  128.7 1.1 fusion.117
  129.8 13.5 %all-to-all-done = bf16[8,96,512]{2,1,0:T(8,128)(2,1)S(1)} async-done(((bf16[8,96,512]{2,1,0:T(8,128)(2,1)}), bf16[8,96,512]{2,1,0:T(8,128)(2,1)S(1)}, u32[]{:S(2)}, u32[]{:S(2)}) %all-to-all-start) | async-done | bytes 786464 | tf_op jit(solution)/shard_map/all_to_all | solution.py:372
  143.4 2.0 gather_fusion
  146.0 1.2 reduce_sum.31
  148.1 2.5 fusion.51
  150.6 1.6 slice.738
  152.2 1.6 slice.703
  153.8 1.6 slice.704
  156.2 1.7 slice.630
  157.8 1.6 slice.623
  159.4 1.6 slice.621
  161.7 1.7 copy.124
  163.4 1.5 slice.631
  164.9 1.5 slice.624
  166.5 1.5 slice.622
  168.0 4.4 %fusion = bf16[1,2048,512]{2,1,0:T(8,128)(2,1)} fusion(bf16[768,2048]{1,0:T(8,128)(2,1)S(1)} %bitcast.309, bf16[768,512]{1,0:T(8,128)(2,1)} %copy-done.22), kind=kOutput, calls=%fused_computation.7 | convolution fusion | flops 1611661312 | bytes 6029312 | tf_op jit(solution)/shard_map/dot_general | solution.py:315
  172.4 3.2 %fusion.1 = bf16[1,2048,512]{2,1,0:T(8,128)(2,1)} fusion(bf16[768,2048]{1,0:T(8,128)(2,1)S(1)} %bitcast.310, bf16[768,512]{1,0:T(8,128)(2,1)S(1)} %copy-done.21), kind=kOutput, calls=%fused_computation.8 | convolution fusion | flops 1611661312 | bytes 6029312 | tf_op jit(solution)/shard_map/dot_general | solution.py:318
  175.5 3.3 %fusion.2 = bf16[1,512,2048]{2,1,0:T(8,128)(2,1)} fusion(bf16[768,2048]{1,0:T(8,128)(2,1)S(1)} %bitcast.365, f32[768,512]{1,0:T(8,128)S(1)} %copy-done.47, f32[768,512]{1,0:T(8,128)S(1)} %copy-done.45), kind=kOutput, calls=%fused_computation.9 | convolution fusion | flops 1614020608 | bytes 8388608 | tf_op jit(solution)/shard_map/dot_general | solution.py:321
  178.9 2.9 %convolution_convert_fusion.3 = bf16[2048,256]{1,0:T(8,128)(2,1)} fusion(bf16[256,2048]{1,0:T(8,128)(2,1)} %all-gather.2.cloned.1.call-done, f32[256,256]{0,1:T(8,128)S(1)} %copy-done.28, bf16[256,256]{0,1:T(8,128)(2,1)S(1)} %copy-done.35), kind=kOutput, calls=%fused_computation.10 | convolution fusion | flops 269680640 | bytes 2490368 | tf_op jit(solution)/shard_map/dot_general | solution.py:393
  181.9 1.3 exponential_multiply_fusion.1
  186.0 1.4 pad.331
  187.4 1.5 pad.258
  188.9 1.4 pad.329
  190.3 1.4 pad.242
  193.6 4.8 %all-to-all-start.1 = ((bf16[8,256,256]{2,1,0:T(8,128)(2,1)}), bf16[8,256,256]{2,1,0:T(8,128)(2,1)S(1)}, u32[]{:S(2)}, u32[]{:S(2)}) async-start(bf16[8,256,256]{2,1,0:T(8,128)(2,1)} %bitcast.313), calls=%async_computation.1 | async-start | bytes 2097152 | tf_op jit(solution)/shard_map/all_to_all | solution.py:397
  198.4 1.5 pad.462
  199.9 1.4 pad.463
  202.1 1.5 pad.211
  204.4 1.7 add_multiply_fusion.2
  206.2 1.0 pad_maximum_fusion.1
  207.3 1.5 pad.226
  211.6 13.3 %share.1 = f32[8,1,1024]{2,1,0:T(1,128)S(1)} custom-call(f32[1,1024]{1,0:T(1,128)S(1)} %bitcast.306), custom_call_target="tpu_custom_call" | custom-call | tf_op jit(solution)/shard_map/share/pallas_call | solution.py:243
  225.1 1.3 multiply_add_fusion
  226.5 1.1 fusion.55
  227.6 1.1 copy.142
  229.0 1.1 copy.146
  230.1 1.8 convolution_add_fusion
  232.7 1.1 add.665
  233.7 1.8 copy.148
  235.5 1.7 rev.8
  237.2 1.3 rev.9
  238.6 1.0 slice_add_fusion
  239.6 1.1 fusion.53
  240.8 1.1 copy.130
  242.3 1.1 convolution_add_fusion.1
  244.2 2.2 add_add_fusion
  246.4 1.8 copy.150
  248.2 1.8 copy.151
  (387 shorter events, 23.5 us)
Async XLA Ops:
  7.2 68.8 %copy-start = (bf16[1,2048,512]{2,1,0:T(8,128)(2,1)S(1)}, bf16[1,2048,512]{2,1,0:T(8,128)(2,1)}, u32[]{:S(2)}) copy-start(bf16[1,2048,512]{2,1,0:T(8,128)(2,1)} %param.20) | copy-start | bytes 6291460
  7.2 5.9 %copy-start.18 = (bf16[256,512]{1,0:T(8,128)(2,1)S(1)}, bf16[256,512]{1,0:T(8,128)(2,1)}, u32[]{:S(2)}) copy-start(bf16[256,512]{1,0:T(8,128)(2,1)} %param.16) | copy-start | bytes 786436
  12.1 3.0 %copy-start.37 = (f32[256,2]{0,1:T(2,128)S(1)}, f32[256,2]{0,1:T(2,128)}, u32[]{:S(2)}) copy-start(f32[256,2]{0,1:T(2,128)} %param.19) | copy-start | bytes 6148
  22.8 1.1 copy-start.2
  76.0 1.8 copy-start.3
  76.0 2.7 %copy-start.14 = (bf16[1,2048,512]{2,1,0:T(8,128)(2,1)S(1)}, bf16[1,2048,512]{2,1,0:T(8,128)(2,1)}, u32[]{:S(2)}) copy-start(bf16[1,2048,512]{2,1,0:T(8,128)(2,1)} %param.21) | copy-start | bytes 6291460
  78.7 1.8 copy-start.44
  78.7 2.5 copy-start.39
  78.7 3.7 %copy-start.41 = (bf16[1,512,2048]{2,1,0:T(8,128)(2,1)S(1)}, bf16[1,512,2048]{2,1,0:T(8,128)(2,1)}, u32[]{:S(2)}) copy-start(bf16[1,512,2048]{2,1,0:T(8,128)(2,1)} %param.22) | copy-start | bytes 6291460
  80.5 4.2 %copy-start.46 = (f32[768,512]{1,0:T(8,128)}, f32[768,512]{1,0:T(8,128)S(1)}, u32[]{:S(2)}) copy-start(f32[768,512]{1,0:T(8,128)S(1)} %fusion.8) | copy-start | bytes 4718596
  84.7 1.9 copy-start.22
  84.7 1.9 copy-start.20
  88.4 35.9 %copy-start.34 = (bf16[256,256]{1,0:T(8,128)(2,1)S(1)}, bf16[256,256]{1,0:T(8,128)(2,1)}, u32[]{:S(2)}) copy-start(bf16[256,256]{1,0:T(8,128)(2,1)} %param.24) | copy-start | bytes 393220
  88.4 35.9 %copy-start.36 = (bf16[2,4,64,64]{3,2,1,0:T(8,128)(2,1)S(1)}, bf16[2,4,64,64]{3,2,1,0:T(8,128)(2,1)}, u32[]{:S(2)}) copy-start(bf16[2,4,64,64]{3,2,1,0:T(8,128)(2,1)} %param.30) | copy-start | bytes 196612
  112.4 12.8 %copy-start.29 = (f32[256,256]{1,0:T(8,128)S(1)}, f32[256,256]{1,0:T(8,128)}, u32[]{:S(2)}) copy-start(f32[256,256]{1,0:T(8,128)} %param.27) | copy-start | bytes 786436
  112.4 31.0 %all-to-all-start = ((bf16[8,96,512]{2,1,0:T(8,128)(2,1)}), bf16[8,96,512]{2,1,0:T(8,128)(2,1)S(1)}, u32[]{:S(2)}, u32[]{:S(2)}) async-start(bf16[8,96,512]{2,1,0:T(8,128)(2,1)} %bitcast.14), calls=%async_computation | async-start | bytes 1572864 | tf_op jit(solution)/shard_map/all_to_all | solution.py:372
  124.3 2.6 %copy-start.30 = (f32[256,256]{1,0:T(8,128)S(1)}, f32[256,256]{1,0:T(8,128)}, u32[]{:S(2)}) copy-start(f32[256,256]{1,0:T(8,128)} %param.26) | copy-start | bytes 786436
  124.3 54.6 %all-gather.2.cloned.1.call-start = ((), (), s32[]{:S(2)}) async-start(), calls=%async_computation.2 | async-start | bytes 1310720 | tf_op jit(solution)/shard_map/all_gather | solution.py:385
  124.3 3.3 %copy-start.31 = (f32[256,256]{1,0:T(8,128)S(1)}, f32[256,256]{1,0:T(8,128)}, u32[]{:S(2)}) copy-start(f32[256,256]{1,0:T(8,128)} %param.28) | copy-start | bytes 786436
  124.6 3.2 %copy-start.32 = (bf16[2,4,64,64]{3,2,1,0:T(8,128)(2,1)S(1)}, bf16[2,4,64,64]{3,2,1,0:T(8,128)(2,1)}, u32[]{:S(2)}) copy-start(bf16[2,4,64,64]{3,2,1,0:T(8,128)(2,1)} %param.29) | copy-start | bytes 196612
  126.8 1.8 copy-start.38
  128.2 17.1 %copy-start.12 = (f32[256,256]{0,1:T(8,128)}, f32[256,256]{0,1:T(8,128)S(1)}, u32[]{:S(2)}) copy-start(f32[256,256]{0,1:T(8,128)S(1)} %copy.119) | copy-start | bytes 786436
  128.7 14.7 %copy-start.10 = (f32[256,256]{0,1:T(8,128)}, f32[256,256]{0,1:T(8,128)S(1)}, u32[]{:S(2)}) copy-start(f32[256,256]{0,1:T(8,128)S(1)} %copy.112) | copy-start | bytes 786436
  145.3 1.9 copy-start.19
  148.1 19.9 %copy-start.4 = (bf16[8,96,2048]{2,1,0:T(8,128)(2,1)S(1)}, bf16[8,96,2048]{2,1,0:T(8,128)(2,1)}, u32[]{:S(2)}) copy-start(bf16[8,96,2048]{2,1,0:T(8,128)(2,1)} %copy-done.3) | copy-start | bytes 9437188
  168.0 4.4 %copy-start.21 = (bf16[768,512]{1,0:T(8,128)(2,1)S(1)}, bf16[768,512]{1,0:T(8,128)(2,1)}, u32[]{:S(2)}) copy-start(bf16[768,512]{1,0:T(8,128)(2,1)} %copy-done.20) | copy-start | bytes 2359300
  172.3 3.2 %copy-start.40 = (bf16[8,96,2048]{2,1,0:T(8,128)(2,1)S(1)}, bf16[8,96,2048]{2,1,0:T(8,128)(2,1)}, u32[]{:S(2)}) copy-start(bf16[8,96,2048]{2,1,0:T(8,128)(2,1)} %get-tuple-element.12) | copy-start | bytes 9437188
  172.3 3.2 %copy-start.45 = (f32[768,512]{1,0:T(8,128)S(1)}, f32[768,512]{1,0:T(8,128)}, u32[]{:S(2)}) copy-start(f32[768,512]{1,0:T(8,128)} %copy-done.44) | copy-start | bytes 4718596
  172.4 3.2 %copy-start.47 = (f32[768,512]{1,0:T(8,128)S(1)}, f32[768,512]{1,0:T(8,128)}, u32[]{:S(2)}) copy-start(f32[768,512]{1,0:T(8,128)} %copy-done.46) | copy-start | bytes 4718596
  175.5 3.3 %copy-start.28 = (f32[256,256]{0,1:T(8,128)S(1)}, f32[256,256]{0,1:T(8,128)}, u32[]{:S(2)}) copy-start(f32[256,256]{0,1:T(8,128)} %fusion.51) | copy-start | bytes 786436
  175.5 3.3 %copy-start.35 = (bf16[256,256]{0,1:T(8,128)(2,1)S(1)}, bf16[256,256]{0,1:T(8,128)(2,1)}, u32[]{:S(2)}) copy-start(bf16[256,256]{0,1:T(8,128)(2,1)} %copy.124) | copy-start | bytes 393220
  178.9 3.0 %copy-start.9 = (f32[256,256]{0,1:T(8,128)S(1)}, f32[256,256]{0,1:T(8,128)}, u32[]{:S(2)}) copy-start(f32[256,256]{0,1:T(8,128)} %get-tuple-element.56) | copy-start | bytes 786436
  178.9 3.0 %copy-start.42 = (bf16[256,2048]{1,0:T(8,128)(2,1)S(1)}, bf16[256,2048]{1,0:T(8,128)(2,1)}, u32[]{:S(2)}) copy-start(bf16[256,2048]{1,0:T(8,128)(2,1)} %param.23) | copy-start | bytes 3145732
  178.9 2.9 %copy-start.43 = (bf16[256,2048]{1,0:T(8,128)(2,1)S(1)}, bf16[256,2048]{1,0:T(8,128)(2,1)}, u32[]{:S(2)}) copy-start(bf16[256,2048]{1,0:T(8,128)(2,1)} %all-gather.2.cloned.1.call-done) | copy-start | bytes 3145732
  181.8 1.3 copy-start.6
  181.8 1.6 copy-start.25
  181.8 1.6 copy-start.26
  183.2 1.8 copy-start.15
  184.9 0.9 copy-start.27
  185.3 0.7 slice-start
  185.8 6.7 %copy-start.23 = (f32[256,128]{0,1:T(8,128)S(1)}, f32[256,128]{0,1:T(8,128)}, u32[]{:S(2)}) copy-start(f32[256,128]{0,1:T(8,128)} %slice.631) | copy-start | bytes 393220
  185.8 6.7 %copy-start.24 = (f32[256,128]{0,1:T(8,128)S(1)}, f32[256,128]{0,1:T(8,128)}, u32[]{:S(2)}) copy-start(f32[256,128]{0,1:T(8,128)} %slice.624) | copy-start | bytes 393220
  193.6 56.4 %all-to-all-start.1 = ((bf16[8,256,256]{2,1,0:T(8,128)(2,1)}), bf16[8,256,256]{2,1,0:T(8,128)(2,1)S(1)}, u32[]{:S(2)}, u32[]{:S(2)}) async-start(bf16[8,256,256]{2,1,0:T(8,128)(2,1)} %bitcast.313), calls=%async_computation.1 | async-start | bytes 2097152 | tf_op jit(solution)/shard_map/all_to_all | solution.py:397
  204.4 22.1 %copy-start.8 = (f32[256,256]{0,1:T(8,128)S(1)}, f32[256,256]{0,1:T(8,128)}, u32[]{:S(2)}) copy-start(f32[256,256]{0,1:T(8,128)} %copy.121) | copy-start | bytes 786436
  204.4 22.1 %copy-start.13 = (f32[256,256]{0,1:T(8,128)S(1)}, f32[256,256]{0,1:T(8,128)}, u32[]{:S(2)}) copy-start(f32[256,256]{0,1:T(8,128)} %copy-done.12) | copy-start | bytes 786436
  206.2 20.2 %copy-start.17 = (f32[256,256]{0,1:T(8,128)}, f32[256,256]{0,1:T(8,128)S(1)}, u32[]{:S(2)}) copy-start(f32[256,256]{0,1:T(8,128)S(1)} %pad.227) | copy-start | bytes 786436
  225.1 3.6 %copy-start.33 = (bf16[2,4,64,64]{3,2,1,0:T(8,128)(2,1)S(1)}, bf16[2,4,64,64]{3,2,1,0:T(8,128)(2,1)}, u32[]{:S(2)}) copy-start(bf16[2,4,64,64]{3,2,1,0:T(8,128)(2,1)} %param.29) | copy-start | bytes 196612
  226.4 5.5 %copy-start.16 = (f32[256,256]{0,1:T(8,128)S(1)}, f32[256,256]{0,1:T(8,128)}, u32[]{:S(2)}) copy-start(f32[256,256]{0,1:T(8,128)} %pad.211) | copy-start | bytes 786436
  231.9 7.7 %copy-start.5 = (f32[256,256]{0,1:T(8,128)S(1)}, f32[256,256]{0,1:T(8,128)}, u32[]{:S(2)}) copy-start(f32[256,256]{0,1:T(8,128)} %copy.116) | copy-start | bytes 786436
  231.9 7.7 %copy-start.7 = (f32[256,256]{0,1:T(8,128)S(1)}, f32[256,256]{0,1:T(8,128)}, u32[]{:S(2)}) copy-start(f32[256,256]{0,1:T(8,128)} %copy.114) | copy-start | bytes 786436
  231.9 7.8 %copy-start.11 = (f32[256,256]{0,1:T(8,128)S(1)}, f32[256,256]{0,1:T(8,128)}, u32[]{:S(2)}) copy-start(f32[256,256]{0,1:T(8,128)} %copy-done.10) | copy-start | bytes 786436
  244.2 6.8 %copy-start.1 = (bf16[1,2048,512]{2,1,0:T(8,128)(2,1)S(1)}, bf16[1,2048,512]{2,1,0:T(8,128)(2,1)}, u32[]{:S(2)}) copy-start(bf16[1,2048,512]{2,1,0:T(8,128)(2,1)} %param.20) | copy-start | bytes 6291460
Sparse Core Ops, SparseCore 0:
  148.2 16.3 all-gather.1
where the time goes:
time: 263 us; the launch traced here: 258 us
  Pallas kernels  89.3 us (34%)
  local copies, waits for them, and re-layouts  66.4 us (25%)
  matrix products  29.1 us (11%)
  other arithmetic  26.8 us (10%)
  starting transfers between devices  16.7 us (6%)
  between operations  16 us (6%)
  waiting for transfers between devices  13.5 us (5%)
    pallas_call x1, Pallas kernels, dispatch(): pl.pallas_call(kernel, name='dispatch', out_shape=(full, full), in_specs=...  52 us
    pallas_call x1, Pallas kernels, scatter_sum(): pl.pallas_call(kernel, name='scatter_sum', out_shape=jax.ShapeDtypeStruct...  24 us
    unnamed x108, local copies, waits for them, and re-layouts  16.1 us
    all_to_all x1, waiting for transfers between devices, on_device(): lax.all_to_all(row_grad.reshape(experts, capacity, width_dev), 'sp', spli...  13.5 us
    pallas_call x1, Pallas kernels, share(): pl.pallas_call(kernel, name='share', out_shape=jax.ShapeDtypeStruct((n,)...  13.3 us
    slice x58, local copies, waits for them, and re-layouts, on_device(): lax.associative_scan(combine_pair, (decay_fwd, decay_fwd * lru_grad), rev...  12.3 us
    all_to_all x1, starting transfers between devices, on_device(): lax.all_to_all(row_grad.reshape(experts, capacity, width_dev), 'sp', spli...  11.9 us
    slice x53, local copies, waits for them, and re-layouts, on_device(): lax.associative_scan(combine_pair, (decay_bwd, decay_bwd * lru_grad), axi...  6.82 us
  transfers between devices with their start and end apart: 3, of which 1 were waited for; matrix products, arithmetic and copies ran while one was open for 29% of the time, Pallas kernels for 5%

commit v1 on v0

v1 whole, which is shorter than its diff:
```python
import jax
import jax.numpy as jnp
from jax import lax
from jax.experimental import pallas as pl
from jax.experimental.pallas import tpu as pltpu
from jax.sharding import PartitionSpec as P

decay_scale = 8.0


MESH = pl.DeviceIdType.MESH
VMEM_SPEC = pl.BlockSpec(memory_space=pltpu.VMEM)


def at(sp=None, tp=None):
    sp = lax.axis_index("sp") if sp is None else sp
    tp = lax.axis_index("tp") if tp is None else tp
    return (sp, tp)


def meet(devices):
    barrier = pltpu.get_barrier_semaphore()
    for device in devices:
        pl.semaphore_signal(barrier, inc=1, device_id=device, device_id_type=MESH)
    pl.semaphore_wait(barrier, len(devices))


def remote(source, target, send, recv, device):
    return pltpu.make_async_remote_copy(
        src_ref=source, dst_ref=target, send_sem=send, recv_sem=recv,
        device_id=device, device_id_type=MESH,
    )


def softplus(value):
    small = jnp.exp(-jnp.abs(value))
    series = small * (1.0 - small * (0.5 - small * (1.0 / 3.0 - small * 0.25)))
    return jnp.maximum(value, 0.0) + jnp.where(small < 0.01, series, jnp.log(1.0 + small))


def one_minus_exp(value, exponential):
    series = -value * (
        1.0 + value * (0.5 + value * (1.0 / 6.0 + value * (1.0 / 24.0 + value * (
            1.0 / 120.0 + value * (1.0 / 720.0)
        ))))
    )
    return jnp.where(value > -0.25, series, 1.0 - exponential)


def layer_backward(
    cotangent, moe_input, routes, gates, w_gate, w_up, w_down, out_proj, conv_in, branch,
    state_before, state_after, jump, recur_weight, input_weight, lam,
):
    n, tp = lax.axis_size("sp"), lax.axis_size("tp")
    chips = tp // 2
    tokens, width = cotangent.shape
    full_width, hidden = w_gate.shape
    cap = -(-(3 * tokens // n) // 16) * 16
    span = min(n, 2 if n <= 8 else 4)
    groups = n // span
    fine = span if n <= 8 else 1
    per_unit = span // fine
    units = groups * fine
    chunk = span * cap
    total_rows = n * cap
    hidden_block = min(hidden, 256)
    column_block = min(full_width, 512)
    grad_block = min(full_width, 256)
    f32, bf16 = jnp.float32, jnp.bfloat16
    channels, length = conv_in.shape
    blocks, block_width = recur_weight.shape[1:3]
    channels_pad = max(channels, 128)
    strip = full_width // n
    upright = strip % 128 == 0
    levels = [1 << i for i in range((length - 1).bit_length())]

    def kernel(
        cot_ref, in_ref, routes_ref, gates_ref, conv_ref, branch_ref, before_ref, after_ref,
        jump_ref, wr_ref, wi_ref, lam_ref, outp_ref, wg_hbm, wu_hbm, wd_hbm,
        res_ref, proj_ref, conv_out, branch_out, gate_hbm, up_hbm, down_hbm,
        wg, wu, wd, key_t, gate_t, pick, send, full, hid, act, part, near, total, far, ret, rets,
        gate_out, up_out, down_out, fullres_ref,
        slopes, steps, decay, tails, speed, mix, gelu_val, gelu_slope, mix_grad, local,
        ends, ends_row, ends_all, carry, proj_part, proj_near, proj_sum, proj_far,
        es, er, xs, xr, zs, zr,
        ws, ss, sr, ys, yr, ps, pr, fs, fr, ns, nr, ts, tr, bs, br, gs, gr, hs, hr, os,
    ):
        me, place = lax.axis_index("sp"), lax.axis_index("tp")
        chip, core = place // 2, place % 2
        partner = chip * 2 + (1 - core)
        group, inner = me // span, me % span

        def columns(member):
            return pl.ds(pl.multiple_of(member * width, width), width)

        mine = columns(place)

        def turned(t, sign):
            return lax.rem(chip + sign * t + chips, chips)

        def across(t, sign):
            return turned(t, sign) * 2 + core

        def order(j):
            return jnp.where(j < 2, j, groups + 1 - j)

        def group_of(j, sign):
            return lax.rem(group + sign * order(j) + groups, groups)

        def peer(j, i, sign):
            return group_of(j, sign) * span + lax.rem(inner + sign * i + span, span)

        weights = ((wg_hbm, wg), (wu_hbm, wu), (wd_hbm, wd))
        loads = [pltpu.make_async_copy(a, b, ws.at[i]) for i, (a, b) in enumerate(weights)]
        for load in loads:
            load.start()

        meet(
            [at(sp=lax.rem(me + k, n)) for k in range(1, n)]
            + [at(tp=partner)]
            + [at(tp=across(t, 1)) for t in range(1, chips)]
        )

        lanes = lax.broadcasted_iota(jnp.int32, (tokens, 128), 1)
        first = lanes == routes_ref[:, 0:1]
        second = lanes == routes_ref[:, 1:2]
        member = jnp.where(first | second, 1.0, 0.0).astype(f32)
        weight = jnp.where(first, gates_ref[:, 0:1], 0.0) + jnp.where(second, gates_ref[:, 1:2], 0.0)
        below = lax.broadcasted_iota(jnp.int32, (tokens, tokens), 1) < lax.broadcasted_iota(
            jnp.int32, (tokens, tokens), 0
        )
        below = jnp.where(below, 1.0, 0.0).astype(bf16)
        position = jnp.dot(below, member.astype(bf16), preferred_element_type=f32)
        key_t[...] = jnp.where(member > 0.5, position, -1.0).T
        gate_t[...] = weight.T
        row_id = lax.broadcasted_iota(jnp.int32, (cap, tokens), 0).astype(f32)

        def packed(to):
            chosen = row_id == key_t[pl.ds(to, 1), :]
            one_hot = jnp.where(chosen, 1.0, 0.0).astype(bf16)
            scale = jnp.sum(jnp.where(chosen, gate_t[pl.ds(to, 1), :], 0.0), axis=1, keepdims=True)
            pick[pl.ds(pl.multiple_of(to * cap, 16), cap), :] = one_hot
            rows = jnp.dot(one_hot, in_ref[...], preferred_element_type=f32).astype(bf16)
            grads = jnp.dot(one_hot, cot_ref[...], preferred_element_type=f32) * scale
            return rows, grads.astype(bf16)

        rows, grads = packed(me)
        full[me, 0, :, mine] = rows
        full[me, 1, :, mine] = grads

        def unit_slice(j, i):
            base = group_of(j, -1) * span
            if fine > 1:
                return pl.ds(base + lax.rem(inner - i + span, span), 1)
            return pl.ds(base, span)

        def dispatch_copy(j, i, sign):
            other = peer(j, i, sign)
            k = j * span + i
            return remote(
                send.at[other], full.at[me if sign > 0 else other, :, :, mine],
                ss.at[k], sr.at[k], at(sp=other),
            )

        def hand_over(j, i):
            block = full.at[unit_slice(j, i), :, :, mine]
            u = j * fine + i
            out = [
                remote(block, block, ys.at[u, t], yr.at[u, t], at(tp=across(t, 1)))
                for t in range(1, chips)
            ]
            out.append(remote(block, block, ps.at[u], pr.at[u], at(tp=partner)))
            return out

        def pass_on(j, i, t):
            block = full.at[unit_slice(j, i), :, :, columns(across(t, -1))]
            u = j * fine + i
            return remote(block, block, fs.at[u, t], fr.at[u, t], at(tp=partner))

        def start_forward(j, begin=0):
            for i in range(begin, fine):
                for s in range(per_unit):
                    number = i * per_unit + s

                    @pl.when(j * span + number > 0)
                    def _():
                        dispatch_copy(j, number, -1).wait_recv()

                for copy in hand_over(j, i):
                    copy.start()

        def start_pass(j):
            for i in range(fine):
                u = j * fine + i
                for t in range(1, chips):
                    block = full.at[unit_slice(j, i), :, :, columns(across(t, -1))]
                    remote(
                        block, block, ys.at[u, t], yr.at[u, t], at(tp=across(t, -1))
                    ).wait_recv()
                    pass_on(j, i, t).start()

        def end_pass(j):
            for i in range(fine):
                u = j * fine + i
                block = full.at[unit_slice(j, i), :, :, columns(partner)]
                remote(block, block, ps.at[u], pr.at[u], at(tp=partner)).wait_recv()
                for t in range(1, chips):
                    block = full.at[
                        unit_slice(j, i), :, :, columns(turned(t, -1) * 2 + (1 - core))
                    ]
                    remote(block, block, fs.at[u, t], fr.at[u, t], at(tp=partner)).wait_recv()

        def chunk_rows(j):
            return pl.ds(pl.multiple_of(group_of(j, -1) * chunk, 16), chunk)

        def near_copy(j, t):
            return remote(
                part.at[chunk_rows(j), columns(turned(t, 1) * 2 + (1 - core))],
                near.at[j, t], ns.at[j, t], nr.at[j, t], at(tp=partner),
            )

        def far_copy(j, t):
            return remote(
                total.at[j, t], far.at[j, t], ts.at[j, t], tr.at[j, t], at(tp=across(t, 1))
            )

        def compute(j):
            base = group_of(j, -1) * span
            where = chunk_rows(j)

            @pl.loop(0, hidden // hidden_block)
            def _(b):
                cut = pl.ds(pl.multiple_of(b * hidden_block, hidden_block), hidden_block)
                rows = full[pl.ds(base, span), 0].reshape(chunk, full_width)
                pre_gate = jnp.dot(rows, wg[:, cut], preferred_element_type=f32)
                pre_up = jnp.dot(rows, wu[:, cut], preferred_element_type=f32)
                grads = full[pl.ds(base, span), 1].reshape(chunk, full_width)
                act_grad = lax.dot_general(
                    grads, wd[cut, :], (((1,), (1,)), ((), ())), preferred_element_type=f32
                )
                sigmoid = jax.nn.sigmoid(pre_gate)
                silu = pre_gate * sigmoid
                slope = sigmoid * (1.0 + pre_gate * (1.0 - sigmoid))
                act[where, cut] = (silu * pre_up).astype(bf16)
                hid[0, where, cut] = (act_grad * pre_up * slope).astype(bf16)
                hid[1, where, cut] = (act_grad * silu).astype(bf16)

            @pl.loop(0, full_width // column_block)
            def _(b):
                cut = pl.ds(pl.multiple_of(b * column_block, column_block), column_block)
                value = lax.dot_general(
                    hid[0, where, :], wg[cut, :], (((1,), (1,)), ((), ())), preferred_element_type=f32
                ) + lax.dot_general(
                    hid[1, where, :], wu[cut, :], (((1,), (1,)), ((), ())), preferred_element_type=f32
                )
                part[where, cut] = value.astype(bf16)

            for t in range(chips):
                near_copy(j, t).start()

        def reduce_near(j):
            where = chunk_rows(j)
            for t in list(range(1, chips)) + [0]:
                near_copy(j, t).wait_recv()
                if t > 0:
                    value = part[where, columns(turned(t, 1) * 2 + core)].astype(f32) + near[
                        j, t
                    ].astype(f32)
                    total[j, t] = value.astype(bf16)
                    far_copy(j, t).start()

        def return_copy(j, i):
            other = peer(j, i, -1)
            k = j * span + i
            return remote(ret.at[other], rets.at[me], bs.at[k], br.at[k], at(sp=other))

        def reduce_far(j):
            where = chunk_rows(j)
            value = part[where, mine].astype(f32) + near[j, 0].astype(f32)
            for t in range(1, chips):
                far_copy(j, t).wait_recv()
                value = value + far[j, t].astype(f32)
            ret[pl.ds(group_of(j, -1) * span, span)] = value.astype(bf16).reshape(span, cap, width)
            for i in range(span):

                @pl.when(j * span + i > 0)
                def _():
                    return_copy(j, i).start()

        if fine > 1:
            for copy in hand_over(0, 0):
                copy.start()

        @pl.loop(1, n)
        def _(k):
            j, i = k // span, k % span
            to = peer(j, i, 1)
            rows, grads = packed(to)
            send[to, 0] = rows
            send[to, 1] = grads
            dispatch_copy(j, i, 1).start()

        start_forward(0, 1 if fine > 1 else 0)

        diagonal = lax.broadcasted_iota(jnp.int32, (channels, channels), 0) == (
            lax.broadcasted_iota(jnp.int32, (channels, channels), 1)
        )
        for d in range(2):
            column = jnp.sum(
                jnp.where(diagonal, lam_ref[d : d + 1, :], 0.0), axis=1, keepdims=True
            )
            speed[d] = decay_scale * softplus(-jnp.broadcast_to(column, (channels, 128)))
        token = lax.broadcasted_iota(jnp.int32, (block_width, length), 1)

        def shifted(value, by, d):
            return pltpu.roll(value, length - by if d == 0 else by, 1)

        def inside(by, d):
            return token < length - by if d == 0 else token >= by

        @pl.loop(0, blocks)
        def _(b):
            rows = pl.ds(pl.multiple_of(b * block_width, block_width), block_width)
            conv = conv_ref[rows, :]
            wide = conv.astype(f32)
            lru_out = jnp.zeros((block_width, length), f32)
            for d, state_ref in enumerate((before_ref, after_ref)):
                recur = jax.nn.sigmoid(
                    lax.dot_general(
                        wr_ref[d, b], conv, (((0,), (0,)), ((), ())), preferred_element_type=f32
                    )
                )
                inward = jax.nn.sigmoid(
                    lax.dot_general(
                        wi_ref[d, b], conv, (((0,), (0,)), ((), ())), preferred_element_type=f32
                    )
                )
                rate = speed[d, rows, 0:1]
                log_decay = jump_ref[rows, :] - rate * recur
                retain = jnp.exp(log_decay)
                root = jnp.sqrt(one_minus_exp(2.0 * log_decay, retain * retain))
                state = state_ref[rows, :]
                lru_out = lru_out + retain * state + root * inward * wide
                log_slope = state * retain - inward * wide * retain * retain / root
                slopes[d, 0, rows, :] = -rate * log_slope * recur * (1.0 - recur)
                slopes[d, 1, rows, :] = root * wide * inward * (1.0 - inward)
                slopes[d, 2, rows, :] = root * inward
                decay[d, rows, :] = retain
                product = retain
                for level, by in enumerate(levels):
                    keep = inside(by, d)
                    steps[d, level, rows, :] = jnp.where(keep, product, 0.0)
                    product = product * jnp.where(keep, shifted(product, by, d), 1.0)
                tails[d, rows, :] = jnp.where(inside(1, d), shifted(product, 1, d), 1.0)
                slopes[d, 3, rows, 0:128] = jnp.broadcast_to(
                    product[:, 0:1] if d == 0 else product[:, length - 1 : length],
                    (block_width, 128),
                )
            value = branch_ref[rows, :].astype(f32)
            scale = 0.7978845608028654
            tanh = jnp.tanh(scale * (value + 0.044715 * value * value * value))
            half = 0.5 * (1.0 + tanh)
            gelu = value * half
            slope = half + 0.5 * value * (1.0 - tanh * tanh) * scale * (
                1.0 + 3.0 * 0.044715 * value * value
            )
            mix[rows, :] = (lru_out * gelu).astype(bf16)
            gelu_val[rows, :] = gelu
            gelu_slope[rows, :] = lru_out * slope

        for load in loads:
            load.wait()

        @pl.loop(0, groups)
        def _(j):
            @pl.when(j < groups - 2)
            def _():
                start_forward(j + 1)

            start_pass(j)

            @pl.when(j > 0)
            def _():
                reduce_near(j - 1)

            end_pass(j)
            compute(j)

            @pl.when(j > 0)
            def _():
                reduce_far(j - 1)

            @pl.when(j == groups - 2)
            def _():
                start_forward(j + 1)

        reduce_near(groups - 1)

        first_contract = (((0,), (0,)), ((), ()))

        @pl.loop(0, full_width // grad_block)
        def _(b):
            cut = pl.ds(pl.multiple_of(b * grad_block, grad_block), grad_block)
            rows = full[:, 0, :, cut].reshape(total_rows, grad_block)
            gate_out[cut, :] = lax.dot_general(
                rows, hid[0], first_contract, preferred_element_type=f32
            ).astype(bf16)
            up_out[cut, :] = lax.dot_general(
                rows, hid[1], first_contract, preferred_element_type=f32
            ).astype(bf16)

        reduce_far(groups - 1)
        rets[me] = ret[me]
        stores = [
            pltpu.make_async_copy(a, b, os.at[i])
            for i, (a, b) in enumerate(
                ((gate_out, gate_hbm), (up_out, up_hbm), (down_out, down_hbm))
            )
        ]
        stores[0].start()
        stores[1].start()

        @pl.loop(0, full_width // grad_block)
        def _(b):
            cut = pl.ds(pl.multiple_of(b * grad_block, grad_block), grad_block)
            grads = full[:, 1, :, cut].reshape(total_rows, grad_block)
            down_out[:, cut] = lax.dot_general(
                act[...], grads, first_contract, preferred_element_type=f32
            ).astype(bf16)

        stores[2].start()

        @pl.loop(1, n)
        def _(k):
            j, i = k // span, k % span
            other = peer(j, i, 1)
            remote(ret.at[other], rets.at[other], bs.at[k], br.at[k], at(sp=other)).wait_recv()

        back = lax.dot_general(
            pick[...], rets[...].reshape(total_rows, width), first_contract,
            preferred_element_type=f32,
        )
        residual = (cot_ref[...].astype(f32) + back).astype(bf16)
        res_ref[...] = residual
        fullres_ref[:, mine] = residual

        def gather_copy(t):
            block = fullres_ref.at[:, mine]
            to = partner if t == 0 else across(t, 1)
            return remote(block, block, gs.at[t], gr.at[t], at(tp=to))

        def gather_pass(t):
            block = fullres_ref.at[:, columns(across(t, -1))]
            return remote(block, block, hs.at[t], hr.at[t], at(tp=partner))

        for t in list(range(1, chips)) + [0]:
            gather_copy(t).start()
        for t in range(1, chips):
            block = fullres_ref.at[:, columns(across(t, -1))]
            remote(block, block, gs.at[t], gr.at[t], at(tp=across(t, -1))).wait_recv()
            gather_pass(t).start()
        block = fullres_ref.at[:, columns(partner)]
        remote(block, block, gs.at[0], gr.at[0], at(tp=partner)).wait_recv()
        for t in range(1, chips):
            block = fullres_ref.at[:, columns(turned(t, -1) * 2 + (1 - core))]
            remote(block, block, hs.at[t], hr.at[t], at(tp=partner)).wait_recv()

        def strip_of(g, i):
            other = g * span + i
            if upright:
                return proj_part.at[:, pl.ds(pl.multiple_of(other * strip, strip), strip)]
            return proj_part.at[pl.ds(pl.multiple_of(other * strip, strip), strip), :]

        def read_strip(other):
            where = pl.ds(pl.multiple_of(other * strip, strip), strip)
            return (proj_part[:, where] if upright else proj_part[where, :]).astype(f32)

        def inner_peer(i, sign):
            return lax.rem(inner + sign * i + span, span)

        def outer_peer(g, sign):
            return lax.rem(group + sign * g + groups, groups)

        def inner_copy(g, i):
            other = outer_peer(g, 1)
            return remote(
                strip_of(other, inner_peer(i, 1)), proj_near.at[g, i], xs.at[g, i], xr.at[g, i],
                at(sp=group * span + inner_peer(i, 1)),
            )

        def outer_copy(g):
            return remote(
                proj_sum.at[g], proj_far.at[g], zs.at[g], zr.at[g],
                at(sp=outer_peer(g, 1) * span + inner),
            )

        turns = list(range(1, groups))
        turns = sorted(turns, key=lambda g: abs(g - groups // 2)) + [0]
        if upright:
            @pl.loop(0, full_width // column_block)
            def _(b):
                cut = pl.ds(pl.multiple_of(b * column_block, column_block), column_block)
                proj_part[:, cut] = jnp.dot(
                    mix[...], fullres_ref[:, cut], preferred_element_type=f32
                ).astype(bf16)
        else:
            @pl.loop(0, full_width // column_block)
            def _(b):
                cut = pl.ds(pl.multiple_of(b * column_block, column_block), column_block)
                proj_part[cut, :] = lax.dot_general(
                    fullres_ref[:, cut], mix[...], (((0,), (1,)), ((), ())),
                    preferred_element_type=f32,
                ).astype(bf16)

        for g in turns:
            for i in range(1, span):
                inner_copy(g, i).start()

        mix_grad[...] = lax.dot_general(
            outp_ref[...], fullres_ref[...], (((1,), (1,)), ((), ())), preferred_element_type=f32
        )
        lane = lax.broadcasted_iota(jnp.int32, (block_width, 128), 1)

        @pl.loop(0, blocks)
        def _(b):
            rows = pl.ds(pl.multiple_of(b * block_width, block_width), block_width)
            upper = mix_grad[rows, :]
            branch_out[rows, :] = upper * gelu_slope[rows, :]
            grad = upper * gelu_val[rows, :]
            last = []
            for d in range(2):
                carried = decay[d, rows, :] * grad
                for level, by in enumerate(levels):
                    carried = carried + steps[d, level, rows, :] * shifted(carried, by, d)
                local[d, rows, :] = grad + jnp.where(inside(1, d), shifted(carried, 1, d), 0.0)
                last.append(carried[:, 0:1] if d == 0 else carried[:, length - 1 : length])
            packed_ends = jnp.where(lane == 0, last[0], jnp.where(lane == 1, last[1], 0.0))
            packed_ends = jnp.where(lane == 2, slopes[0, 3, rows, 0:128], packed_ends)
            ends[rows, :] = jnp.where(lane == 3, slopes[1, 3, rows, 0:128], packed_ends)

        if channels < channels_pad:
            ends[channels:, :] = jnp.zeros((channels_pad - channels, 128), f32)
        ends_row[...] = ends[...].T[0:8, :]

        def ends_copy(k):
            return remote(
                ends_row, ends_all.at[me], es.at[k], er.at[k], at(sp=lax.rem(me + k, n))
            )

        @pl.loop(1, n)
        def _(k):
            ends_copy(k).start()

        ends_all[me] = ends_row[...]

        for g in turns:
            total_strip = read_strip(outer_peer(g, 1) * span + inner)
            for i in range(1, span):
                inner_copy(g, i).wait_recv()
                total_strip = total_strip + proj_near[g, i].astype(f32)
            proj_sum[g] = total_strip.astype(bf16)
            if g > 0:
                outer_copy(g).start()

        @pl.loop(1, n)
        def _(k):
            origin = lax.rem(me - k + n, n)
            remote(
                ends_row, ends_all.at[origin], es.at[k], er.at[k], at(sp=origin)
            ).wait_recv()

        incoming = [jnp.zeros((1, channels_pad), f32)] * 2
        for turn in range(n - 1):
            late = n - 1 - turn
            incoming[0] = jnp.where(
                late > me, ends_all[late, 2:3, :] * incoming[0] + ends_all[late, 0:1, :], incoming[0]
            )
            incoming[1] = jnp.where(
                turn < me, ends_all[turn, 3:4, :] * incoming[1] + ends_all[turn, 1:2, :], incoming[1]
            )
        line = lax.broadcasted_iota(jnp.int32, (128, channels_pad), 0)
        carry[...] = jnp.where(line == 0, incoming[0], jnp.where(line == 1, incoming[1], 0.0)).T

        @pl.loop(0, blocks)
        def _(b):
            rows = pl.ds(pl.multiple_of(b * block_width, block_width), block_width)
            value = jnp.zeros((block_width, length), f32)
            for d in range(2):
                delta = local[d, rows, :] + tails[d, rows, :] * carry[rows, d : d + 1]
                value = value + delta * slopes[d, 2, rows, :]
                value = value + jnp.dot(
                    wr_ref[d, b], (delta * slopes[d, 0, rows, :]).astype(bf16),
                    preferred_element_type=f32,
                )
                value = value + jnp.dot(
                    wi_ref[d, b], (delta * slopes[d, 1, rows, :]).astype(bf16),
                    preferred_element_type=f32,
                )
            conv_out[rows, :] = value

        summed = proj_sum[0].astype(f32)
        for g in turns[:-1]:
            outer_copy(g).wait_recv()
            summed = summed + proj_far[g].astype(f32)
        proj_ref[...] = summed if upright else summed.T

        for g in turns:
            for i in range(1, span):
                inner_copy(g, i).wait_send()
            if g > 0:
                outer_copy(g).wait_send()

        @pl.loop(1, n)
        def _(k):
            ends_copy(k).wait_send()

        @pl.loop(1, n)
        def _(k):
            j, i = k // span, k % span
            dispatch_copy(j, i, 1).wait_send()
            return_copy(j, i).wait_send()

        @pl.loop(0, groups)
        def _(j):
            for i in range(fine):
                for copy in hand_over(j, i):
                    copy.wait_send()
                for t in range(1, chips):
                    pass_on(j, i, t).wait_send()
            for t in range(chips):
                near_copy(j, t).wait_send()
            for t in range(1, chips):
                far_copy(j, t).wait_send()

        for t in range(chips):
            gather_copy(t).wait_send()
        for t in range(1, chips):
            gather_pass(t).wait_send()
        for store in stores:
            store.wait()

    dma = pltpu.SemaphoreType.DMA
    wide = max(chips, 2)
    sem = lambda *shape: [dma(shape)] * 2
    any_spec = pl.BlockSpec(memory_space=pl.ANY)
    shape = jax.ShapeDtypeStruct
    strip_shape = (channels, strip) if upright else (strip, channels)
    part_shape = (channels, full_width) if upright else (full_width, channels)
    return pl.pallas_call(
        kernel, name="layer_backward",
        out_shape=(
            shape((tokens, width), bf16), shape((channels, strip), f32),
            shape((channels, length), f32), shape((channels, length), f32),
            shape(w_gate.shape, bf16), shape(w_up.shape, bf16), shape(w_down.shape, bf16),
        ),
        in_specs=[VMEM_SPEC] * 13 + [any_spec] * 3,
        out_specs=(VMEM_SPEC,) * 4 + (any_spec,) * 3,
        scratch_shapes=[
            pltpu.VMEM(w_gate.shape, bf16), pltpu.VMEM(w_up.shape, bf16), pltpu.VMEM(w_down.shape, bf16),
            pltpu.VMEM((128, tokens), f32), pltpu.VMEM((128, tokens), f32),
            pltpu.VMEM((total_rows, tokens), bf16),
            pltpu.VMEM((n, 2, cap, width), bf16),
            pltpu.VMEM((n, 2, cap, full_width), bf16),
            pltpu.VMEM((2, total_rows, hidden), bf16),
            pltpu.VMEM((total_rows, hidden), bf16),
            pltpu.VMEM((total_rows, full_width), bf16),
            pltpu.VMEM((groups, chips, chunk, width), bf16),
            pltpu.VMEM((groups, chips, chunk, width), bf16),
            pltpu.VMEM((groups, chips, chunk, width), bf16),
            pltpu.VMEM((n, cap, width), bf16), pltpu.VMEM((n, cap, width), bf16),
            pltpu.VMEM(w_gate.shape, bf16), pltpu.VMEM(w_up.shape, bf16), pltpu.VMEM(w_down.shape, bf16),
            pltpu.VMEM((tokens, full_width), bf16),
            pltpu.VMEM((2, 4, channels, length), f32),
            pltpu.VMEM((2, len(levels), channels, length), f32),
            pltpu.VMEM((2, channels, length), f32), pltpu.VMEM((2, channels, length), f32),
            pltpu.VMEM((2, channels, 128), f32),
            pltpu.VMEM((channels, length), bf16),
            pltpu.VMEM((channels, length), f32), pltpu.VMEM((channels, length), f32),
            pltpu.VMEM((channels, length), f32), pltpu.VMEM((2, channels, length), f32),
            pltpu.VMEM((channels_pad, 128), f32), pltpu.VMEM((8, channels_pad), f32),
            pltpu.VMEM((n, 8, channels_pad), f32), pltpu.VMEM((channels_pad, 128), f32),
            pltpu.VMEM(part_shape, bf16),
            pltpu.VMEM((groups, span) + strip_shape, bf16),
            pltpu.VMEM((groups,) + strip_shape, bf16), pltpu.VMEM((groups,) + strip_shape, bf16),
        ]
        + sem(n) + sem(groups, span) + sem(groups)
        + [dma((3,))]
        + sem(n) + sem(units, wide) + sem(units) + sem(units, wide)
        + sem(groups, wide) + sem(groups, wide) + sem(n) + sem(wide) + sem(wide) + [dma((3,))],
        compiler_params=pltpu.CompilerParams(
            collective_id=1, has_side_effects=True, vmem_limit_bytes=60 * 1024 * 1024
        ),
    )(
        cotangent, moe_input, routes, gates, conv_in, branch, state_before, state_after, jump,
        recur_weight, input_weight, lam, out_proj, w_gate, w_up, w_down,
    )


def on_device(
    cotangent, moe_input, routes, gates, w_gate, w_up, w_down, out_proj, conv_in, branch,
    state_before, state_after, jump, recur_weight, input_weight, lam,
):
    residual_grad, out_proj_grad, conv_grad, branch_grad, gate_grad, up_grad, down_grad = (
        layer_backward(
            cotangent, moe_input, routes, gates, w_gate[0], w_up[0], w_down[0], out_proj, conv_in,
            branch, state_before, state_after, jump, recur_weight, input_weight, lam,
        )
    )
    return (
        gate_grad[None], up_grad[None], down_grad[None],
        residual_grad, out_proj_grad, conv_grad, branch_grad,
    )


def solution(mesh):
    placed = (
        P("sp", "tp"),
        P("sp", "tp"),
        P("sp", None),
        P("sp", None),
        P("sp", None, "tp"),
        P("sp", None, "tp"),
        P("sp", "tp", None),
        P("tp", None),
        P("tp", "sp"),
        P("tp", "sp"),
        P("tp", "sp"),
        P("tp", "sp"),
        P("tp", "sp"),
        P(None, "tp", None, None),
        P(None, "tp", None, None),
        P(None, "tp"),
    )
    return jax.shard_map(
        on_device,
        mesh=mesh,
        in_specs=placed,
        out_specs=(
            P("sp", None, "tp"),
            P("sp", None, "tp"),
            P("sp", "tp", None),
            P("sp", "tp"),
            P("tp", "sp"),
            P("tp", "sp"),
            P("tp", "sp"),
        ),
        check_vma=False,
    )
```

time: 263 us -> 129 us (0.49); the launches traced: 258 us -> 128 us
  local copies, waits for them, and re-layouts: 66.4 us -> 12.6 us
  matrix products: 29.1 us -> 0 us
  other arithmetic: 26.8 us -> 0 us
  Pallas kernels: 89.3 us -> 114 us
  starting transfers between devices: 16.7 us -> 0 us
  between operations: 16 us -> 0.66 us
  waiting for transfers between devices: 13.5 us -> 0 us
    dot_general x18 -> x0, matrix products: 29.1 us -> none  [the longest x1 4.36 us: expert_pass(): lax.dot_general(full_rows, gate_hidden, contract_first, preferred_element...]
    pallas_call x3 -> x1, Pallas kernels: 89.3 us -> 114 us  [layer_backward(): pl.pallas_call(kernel, name='layer_backward', out_shape=(shape((tokens, w...]
    slice x116 -> x0, local copies, waits for them, and re-layouts: 22.2 us -> none  [the longest x58 12.3 us: on_device(): lax.associative_scan(combine_pair, (decay_fwd, decay_fwd * lru_grad), rev...]
    all_to_all x2 -> x0, starting transfers between devices: 16.6 us -> none  [the longest x1 11.9 us: on_device(): lax.all_to_all(row_grad.reshape(experts, capacity, width_dev), 'sp', spli...]
    all_to_all x2 -> x0, waiting for transfers between devices: 13.5 us -> none  [the longest x1 13.5 us: on_device(): lax.all_to_all(row_grad.reshape(experts, capacity, width_dev), 'sp', spli...]
    add x38 -> x0, other arithmetic: 11.9 us -> none  [the longest x18 3.32 us: on_device(): lax.associative_scan(combine_pair, (decay_fwd, decay_fwd * lru_grad), rev...]
    pad x54 -> x0, local copies, waits for them, and re-layouts: 6.45 us -> none  [the longest x28 3.27 us: on_device(): lax.associative_scan(combine_pair, (decay_fwd, decay_fwd * lru_grad), rev...]
    mul x9 -> x0, local copies, waits for them, and re-layouts: 5.75 us -> none  [the longest x2 2.15 us: gate_backward(): recur_grad = log_grad * -speed_row * recur_gate * (1.0 - recur_gate)]
  transfers between devices with their start and end apart: 3 -> 0, of which waited for: 1 -> 0; matrix products, arithmetic and copies ran while one was open for 29% -> 0% of each run, Pallas kernels for 5% -> 0%
where the time goes in v1:
time: 129 us; the launch traced here: 128 us
  Pallas kernels  114 us (88%)
  local copies, waits for them, and re-layouts  12.6 us (10%)
    pallas_call x1, Pallas kernels, layer_backward(): pl.pallas_call(kernel, name='layer_backward', out_shape=(shape((tokens, w...  114 us
    unnamed x21, local copies, waits for them, and re-layouts  12.6 us

profile of v1, /device:TPU:5, one launch (start us, length us, event | category | flops | bytes accessed | tf_op | source)
XLA Modules:
  0.0 127.7 jit_solution(10786437347266511766)
XLA Ops:
  0.6 1.5 %copy.23.routes_ref = s32[256,2]{1,0:T(8,128)} copy(s32[256,2]{0,1:T(2,128)} %param.18) | data formatting | bytes 4096 | tf_op args[2]
  2.1 1.5 %copy.24.gates_ref = f32[256,2]{1,0:T(8,128)} copy(f32[256,2]{0,1:T(2,128)} %param.19) | data formatting | bytes 4096 | tf_op args[3]
  3.6 114.4 %layer_backward.1 = (bf16[256,512]{1,0:T(8,128)(2,1)}, f32[256,256]{1,0:T(8,128)}, f32[256,256]{1,0:T(8,128)}, f32[256,256]{1,0:T(8,128)}, bf16[2048,512]{1,0:T(...) custom-call(bf16[256,512]{1,0:T(8,128)(2,1)} %cot_ref.1, bf16[256,512]{1,0:T(8,128)(2,1)} %in_ref.1, ...), custom_call_target="tpu_custom_call" | custom-call | tf_op jit(solution)/shard_map/layer_backward/pallas_call | solution.py:649
  118.0 0.0 copy-start.1
  118.0 3.2 %copy.32 = bf16[1,2048,512]{2,1,0:T(8,128)(2,1)} copy(bf16[1,2048,512]{2,1,0:T(8,128)(2,1)} %bitcast.11) | data formatting | bytes 4194304
  121.2 0.0 copy-done.1
  121.2 0.0 copy-start
  121.2 1.3 %copy.33 = bf16[1,2048,512]{2,1,0:T(8,128)(2,1)} copy(bf16[1,2048,512]{2,1,0:T(8,128)(2,1)S(1)} %bitcast.10) | data formatting | bytes 4194304
  122.5 1.0 copy-done
  123.5 0.0 copy-start.5
  123.5 0.0 copy-start.4
  123.5 0.0 copy-start.3
  123.5 0.0 copy-start.2
  123.5 1.3 %copy.34 = bf16[1,512,2048]{2,1,0:T(8,128)(2,1)} copy(bf16[1,512,2048]{2,1,0:T(8,128)(2,1)S(1)} %bitcast.9) | data formatting | bytes 4194304
  124.8 0.0 copy-done.5
  124.8 0.7 copy.35
  125.5 0.0 copy-done.4
  125.5 0.7 copy.36
  126.3 0.0 copy-done.3
  126.3 0.7 copy.37
  127.0 0.0 copy-done.2
  127.0 0.7 copy.38
Async XLA Ops:
  118.0 3.2 %copy-start.1 = (bf16[2048,512]{1,0:T(8,128)(2,1)S(1)}, bf16[2048,512]{1,0:T(8,128)(2,1)}, u32[]{:S(2)}) copy-start(bf16[2048,512]{1,0:T(8,128)(2,1)} %get-tuple-element.15) | copy-start | bytes 6291460
  121.2 2.3 %copy-start = (bf16[512,2048]{1,0:T(8,128)(2,1)S(1)}, bf16[512,2048]{1,0:T(8,128)(2,1)}, u32[]{:S(2)}) copy-start(bf16[512,2048]{1,0:T(8,128)(2,1)} %get-tuple-element.16) | copy-start | bytes 6291460
  123.5 1.3 %copy-start.5 = (bf16[256,512]{1,0:T(8,128)(2,1)S(1)}, bf16[256,512]{1,0:T(8,128)(2,1)}, u32[]{:S(2)}) copy-start(bf16[256,512]{1,0:T(8,128)(2,1)} %get-tuple-element.31) | copy-start | bytes 786436
  123.5 2.0 %copy-start.4 = (f32[256,256]{1,0:T(8,128)S(1)}, f32[256,256]{1,0:T(8,128)}, u32[]{:S(2)}) copy-start(f32[256,256]{1,0:T(8,128)} %get-tuple-element.32) | copy-start | bytes 786436
  123.5 2.7 %copy-start.3 = (f32[256,256]{1,0:T(8,128)S(1)}, f32[256,256]{1,0:T(8,128)}, u32[]{:S(2)}) copy-start(f32[256,256]{1,0:T(8,128)} %get-tuple-element.33) | copy-start | bytes 786436
  123.5 3.4 %copy-start.2 = (f32[256,256]{1,0:T(8,128)S(1)}, f32[256,256]{1,0:T(8,128)}, u32[]{:S(2)}) copy-start(f32[256,256]{1,0:T(8,128)} %get-tuple-element.34) | copy-start | bytes 786436

commit v2 on v1

--- a/solution.py
+++ b/solution.py
@@ -77,13 +77,13 @@
     def kernel(
         cot_ref, in_ref, routes_ref, gates_ref, conv_ref, branch_ref, before_ref, after_ref,
         jump_ref, wr_ref, wi_ref, lam_ref, outp_ref, wg_hbm, wu_hbm, wd_hbm,
-        res_ref, proj_ref, conv_out, branch_out, gate_hbm, up_hbm, down_hbm,
+        res_ref, proj_ref, conv_out, branch_out, gate_out, up_out, down_out,
         wg, wu, wd, key_t, gate_t, pick, send, full, hid, act, part, near, total, far, ret, rets,
-        gate_out, up_out, down_out, fullres_ref,
+        fullres_ref,
         slopes, steps, decay, tails, speed, mix, gelu_val, gelu_slope, mix_grad, local,
         ends, ends_row, ends_all, carry, proj_part, proj_near, proj_sum, proj_far,
         es, er, xs, xr, zs, zr,
-        ws, ss, sr, ys, yr, ps, pr, fs, fr, ns, nr, ts, tr, bs, br, gs, gr, hs, hr, os,
+        ws, ss, sr, ys, yr, ps, pr, fs, fr, ns, nr, ts, tr, bs, br, gs, gr, hs, hr,
     ):
         me, place = lax.axis_index("sp"), lax.axis_index("tp")
         chip, core = place // 2, place % 2
@@ -121,18 +121,19 @@
             + [at(tp=across(t, 1)) for t in range(1, chips)]
         )
 
-        lanes = lax.broadcasted_iota(jnp.int32, (tokens, 128), 1)
-        first = lanes == routes_ref[:, 0:1]
-        second = lanes == routes_ref[:, 1:2]
+        expert_id = lax.broadcasted_iota(jnp.int32, (128, tokens), 0)
+        first = expert_id == routes_ref[0:1, :]
+        second = expert_id == routes_ref[1:2, :]
         member = jnp.where(first | second, 1.0, 0.0).astype(f32)
-        weight = jnp.where(first, gates_ref[:, 0:1], 0.0) + jnp.where(second, gates_ref[:, 1:2], 0.0)
-        below = lax.broadcasted_iota(jnp.int32, (tokens, tokens), 1) < lax.broadcasted_iota(
-            jnp.int32, (tokens, tokens), 0
+        gate_t[...] = jnp.where(first, gates_ref[0:1, :], 0.0) + jnp.where(
+            second, gates_ref[1:2, :], 0.0
         )
-        below = jnp.where(below, 1.0, 0.0).astype(bf16)
-        position = jnp.dot(below, member.astype(bf16), preferred_element_type=f32)
-        key_t[...] = jnp.where(member > 0.5, position, -1.0).T
-        gate_t[...] = weight.T
+        earlier = lax.broadcasted_iota(jnp.int32, (tokens, tokens), 0) < lax.broadcasted_iota(
+            jnp.int32, (tokens, tokens), 1
+        )
+        earlier = jnp.where(earlier, 1.0, 0.0).astype(bf16)
+        position = jnp.dot(member.astype(bf16), earlier, preferred_element_type=f32)
+        key_t[...] = jnp.where(member > 0.5, position, -1.0)
         row_id = lax.broadcasted_iota(jnp.int32, (cap, tokens), 0).astype(f32)
 
         def packed(to):
@@ -177,8 +178,8 @@
             u = j * fine + i
             return remote(block, block, fs.at[u, t], fr.at[u, t], at(tp=partner))
 
-        def start_forward(j, begin=0):
-            for i in range(begin, fine):
+        def start_forward(j, begin=0, end=fine):
+            for i in range(begin, min(end, fine)):
                 for s in range(per_unit):
                     number = i * per_unit + s
 
@@ -188,6 +189,14 @@
 
                 for copy in hand_over(j, i):
                     copy.start()
+
+        half = span // 2
+
+        def release(j, begin, end):
+            @pl.when(j < groups)
+            def _():
+                for i in range(begin, end):
+                    dispatch_copy(j, i, 1).start()
 
         def start_pass(j):
             for i in range(fine):
@@ -298,9 +307,13 @@
             rows, grads = packed(to)
             send[to, 0] = rows
             send[to, 1] = grads
-            dispatch_copy(j, i, 1).start()
+
+            @pl.when(j < 2)
+            def _():
+                dispatch_copy(j, i, 1).start()
 
         start_forward(0, 1 if fine > 1 else 0)
+        release(2, 0, span)
 
         diagonal = lax.broadcasted_iota(jnp.int32, (channels, channels), 0) == (
             lax.broadcasted_iota(jnp.int32, (channels, channels), 1)
@@ -376,26 +389,34 @@
             @pl.when(j < groups - 2)
             def _():
                 start_forward(j + 1)
+                release(j + 3, 0, half)
+
+            @pl.when((j > 0) & (j < groups - 2))
+            def _():
+                release(j + 2, half, span)
 
             start_pass(j)
-
-            @pl.when(j > 0)
-            def _():
-                reduce_near(j - 1)
-
             end_pass(j)
             compute(j)
 
-            @pl.when(j > 0)
+            @pl.when(j == groups - 2)
+            def _():
+                start_forward(groups - 1, 1)
+
+            @pl.when((j > 0) & (j < groups - 1))
+            def _():
+                reduce_near(j)
+
+            @pl.when(j == groups - 3)
+            def _():
+                start_forward(groups - 1, 0, 1)
+
+            @pl.when(j > 1)
             def _():
                 reduce_far(j - 1)
 
-            @pl.when(j == groups - 2)
-            def _():
-                start_forward(j + 1)
-
         reduce_near(groups - 1)
-
+        reduce_near(0)
         first_contract = (((0,), (0,)), ((), ()))
 
         @pl.loop(0, full_width // grad_block)
@@ -410,16 +431,6 @@
             ).astype(bf16)
 
         reduce_far(groups - 1)
-        rets[me] = ret[me]
-        stores = [
-            pltpu.make_async_copy(a, b, os.at[i])
-            for i, (a, b) in enumerate(
-                ((gate_out, gate_hbm), (up_out, up_hbm), (down_out, down_hbm))
-            )
-        ]
-        stores[0].start()
-        stores[1].start()
-
         @pl.loop(0, full_width // grad_block)
         def _(b):
             cut = pl.ds(pl.multiple_of(b * grad_block, grad_block), grad_block)
@@ -428,7 +439,8 @@
                 act[...], grads, first_contract, preferred_element_type=f32
             ).astype(bf16)
 
-        stores[2].start()
+        reduce_far(0)
+        rets[me] = ret[me]
 
         @pl.loop(1, n)
         def _(k):
@@ -496,26 +508,32 @@
 
         turns = list(range(1, groups))
         turns = sorted(turns, key=lambda g: abs(g - groups // 2)) + [0]
-        if upright:
-            @pl.loop(0, full_width // column_block)
-            def _(b):
-                cut = pl.ds(pl.multiple_of(b * column_block, column_block), column_block)
-                proj_part[:, cut] = jnp.dot(
-                    mix[...], fullres_ref[:, cut], preferred_element_type=f32
+        turn_width = span * strip
+
+        def project(g):
+            where = pl.ds(pl.multiple_of(outer_peer(g, 1) * turn_width, turn_width), turn_width)
+            if upright:
+                proj_part[:, where] = jnp.dot(
+                    mix[...], fullres_ref[:, where], preferred_element_type=f32
                 ).astype(bf16)
-        else:
-            @pl.loop(0, full_width // column_block)
-            def _(b):
-                cut = pl.ds(pl.multiple_of(b * column_block, column_block), column_block)
-                proj_part[cut, :] = lax.dot_general(
-                    fullres_ref[:, cut], mix[...], (((0,), (1,)), ((), ())),
+            else:
+                proj_part[where, :] = lax.dot_general(
+                    fullres_ref[:, where], mix[...], (((0,), (1,)), ((), ())),
                     preferred_element_type=f32,
                 ).astype(bf16)
-
-        for g in turns:
             for i in range(1, span):
                 inner_copy(g, i).start()
 
+        def finish_inner(g):
+            total_strip = read_strip(outer_peer(g, 1) * span + inner)
+            for i in range(1, span):
+                inner_copy(g, i).wait_recv()
+                total_strip = total_strip + proj_near[g, i].astype(f32)
+            proj_sum[g] = total_strip.astype(bf16)
+            if g > 0:
+                outer_copy(g).start()
+
+        project(turns[0])
         mix_grad[...] = lax.dot_general(
             outp_ref[...], fullres_ref[...], (((1,), (1,)), ((), ())), preferred_element_type=f32
         )
@@ -553,15 +571,10 @@
 
         ends_all[me] = ends_row[...]
 
-        for g in turns:
-            total_strip = read_strip(outer_peer(g, 1) * span + inner)
-            for i in range(1, span):
-                inner_copy(g, i).wait_recv()
-                total_strip = total_strip + proj_near[g, i].astype(f32)
-            proj_sum[g] = total_strip.astype(bf16)
-            if g > 0:
-                outer_copy(g).start()
-
+        for g in turns[1:]:
+            project(g)
+        for g in turns[:-2]:
+            finish_inner(g)
         @pl.loop(1, n)
         def _(k):
             origin = lax.rem(me - k + n, n)
@@ -598,6 +611,8 @@
                 )
             conv_out[rows, :] = value
 
+        for g in turns[-2:]:
+            finish_inner(g)
         summed = proj_sum[0].astype(f32)
         for g in turns[:-1]:
             outer_copy(g).wait_recv()
@@ -636,8 +651,7 @@
             gather_copy(t).wait_send()
         for t in range(1, chips):
             gather_pass(t).wait_send()
-        for store in stores:
-            store.wait()
+
 
     dma = pltpu.SemaphoreType.DMA
     wide = max(chips, 2)
@@ -649,12 +663,12 @@
     return pl.pallas_call(
         kernel, name="layer_backward",
         out_shape=(
-            shape((tokens, width), bf16), shape((channels, strip), f32),
-            shape((channels, length), f32), shape((channels, length), f32),
-            shape(w_gate.shape, bf16), shape(w_up.shape, bf16), shape(w_down.shape, bf16),
+            pltpu.VMEM((tokens, width), bf16), pltpu.VMEM((channels, strip), f32),
+            pltpu.VMEM((channels, length), f32), pltpu.VMEM((channels, length), f32),
+            pltpu.VMEM(w_gate.shape, bf16), pltpu.VMEM(w_up.shape, bf16), pltpu.VMEM(w_down.shape, bf16),
         ),
         in_specs=[VMEM_SPEC] * 13 + [any_spec] * 3,
-        out_specs=(VMEM_SPEC,) * 4 + (any_spec,) * 3,
+        out_specs=(VMEM_SPEC,) * 7,
         scratch_shapes=[
             pltpu.VMEM(w_gate.shape, bf16), pltpu.VMEM(w_up.shape, bf16), pltpu.VMEM(w_down.shape, bf16),
             pltpu.VMEM((128, tokens), f32), pltpu.VMEM((128, tokens), f32),
@@ -668,7 +682,6 @@
             pltpu.VMEM((groups, chips, chunk, width), bf16),
             pltpu.VMEM((groups, chips, chunk, width), bf16),
             pltpu.VMEM((n, cap, width), bf16), pltpu.VMEM((n, cap, width), bf16),
-            pltpu.VMEM(w_gate.shape, bf16), pltpu.VMEM(w_up.shape, bf16), pltpu.VMEM(w_down.shape, bf16),
             pltpu.VMEM((tokens, full_width), bf16),
             pltpu.VMEM((2, 4, channels, length), f32),
             pltpu.VMEM((2, len(levels), channels, length), f32),
@@ -686,14 +699,37 @@
         + sem(n) + sem(groups, span) + sem(groups)
         + [dma((3,))]
         + sem(n) + sem(units, wide) + sem(units) + sem(units, wide)
-        + sem(groups, wide) + sem(groups, wide) + sem(n) + sem(wide) + sem(wide) + [dma((3,))],
+        + sem(groups, wide) + sem(groups, wide) + sem(n) + sem(wide) + sem(wide),
         compiler_params=pltpu.CompilerParams(
-            collective_id=1, has_side_effects=True, vmem_limit_bytes=60 * 1024 * 1024
+            collective_id=1, has_side_effects=True, vmem_limit_bytes=54 * 1024 * 1024
         ),
     )(
-        cotangent, moe_input, routes, gates, conv_in, branch, state_before, state_after, jump,
+        cotangent, moe_input, routes.T, gates.T, conv_in, branch, state_before, state_after, jump,
         recur_weight, input_weight, lam, out_proj, w_gate, w_up, w_down,
     )
+
+
+def write_out(values):
+    count = len(values)
+
+    def kernel(*refs):
+        sems = refs[2 * count]
+        copies = [
+            pltpu.make_async_copy(refs[i], refs[count + i], sems.at[i]) for i in range(count)
+        ]
+        for copy in copies:
+            copy.start()
+        for copy in copies:
+            copy.wait()
+
+    return pl.pallas_call(
+        kernel, name="write_out",
+        out_shape=tuple(jax.ShapeDtypeStruct(v.shape, v.dtype) for v in values),
+        in_specs=[pl.BlockSpec(memory_space=pl.ANY)] * count,
+        out_specs=(pl.BlockSpec(memory_space=pl.ANY),) * count,
+        scratch_shapes=[pltpu.SemaphoreType.DMA((count,))],
+        compiler_params=pltpu.CompilerParams(vmem_limit_bytes=4 * 1024 * 1024),
+    )(*values)
 
 
 def on_device(
@@ -701,10 +737,10 @@
     state_before, state_after, jump, recur_weight, input_weight, lam,
 ):
     residual_grad, out_proj_grad, conv_grad, branch_grad, gate_grad, up_grad, down_grad = (
-        layer_backward(
+        write_out(layer_backward(
             cotangent, moe_input, routes, gates, w_gate[0], w_up[0], w_down[0], out_proj, conv_in,
             branch, state_before, state_after, jump, recur_weight, input_weight, lam,
-        )
+        ))
     )
     return (
         gate_grad[None], up_grad[None], down_grad[None],

time: 129 us -> 105 us (0.81)
  local copies, waits for them, and re-layouts: 12.6 us -> 0 us
  Pallas kernels: 114 us -> 103 us
    unnamed x21 -> x0, local copies, waits for them, and re-layouts: 12.6 us -> none
    pallas_call x1 -> x2, Pallas kernels: 114 us -> 103 us  [the longest x1 99.7 us: layer_backward(): pl.pallas_call(kernel, name='layer_backward', out_shape=(pltpu.VMEM((toke...]
where the time goes in v2:
time: 105 us; the launch traced here: 103 us
  Pallas kernels  103 us (98%)
    pallas_call x1, Pallas kernels, layer_backward(): pl.pallas_call(kernel, name='layer_backward', out_shape=(pltpu.VMEM((toke...  99.7 us
    pallas_call x1, Pallas kernels, write_out(): pl.pallas_call(kernel, name='write_out', out_shape=tuple((jax.ShapeDtypeS...  3.11 us

profile of v2, /device:TPU:5, one launch (start us, length us, event | category | flops | bytes accessed | tf_op | source)
XLA Modules:
  0.0 103.5 jit_solution(14847732208382817437)
XLA Ops:
  0.6 99.7 %layer_backward.1 = (bf16[256,512]{1,0:T(8,128)(2,1)S(1)}, f32[256,256]{1,0:T(8,128)S(1)}, f32[256,256]{1,0:T(8,128)S(1)}, f32[256,256]{1,0:T(8,128)S(1)}, bf16[...) custom-call(bf16[256,512]{1,0:T(8,128)(2,1)} %cot_ref.1, ...), custom_call_target="tpu_custom_call" | custom-call | tf_op jit(solution)/shard_map/layer_backward/pallas_call | solution.py:663
  100.3 3.1 %write_out.1 = (bf16[256,512]{1,0:T(8,128)(2,1)}, f32[256,256]{1,0:T(8,128)}, f32[256,256]{1,0:T(8,128)}, f32[256,256]{1,0:T(8,128)}, bf16[2048,512]{1,0:T(8,128...) custom-call(bf16[256,512]{1,0:T(8,128)(2,1)S(1)} %get-tuple-element.21.refs_0_, ...), custom_call_target="tpu_custom_call" | custom-call | tf_op jit(solution)/shard_map/write_out/pallas_call | solution.py:725

commit v3 on v2

--- a/solution.py
+++ b/solution.py
@@ -63,6 +63,9 @@
     units = groups * fine
     chunk = span * cap
     total_rows = n * cap
+    pieces = 2 if span % 2 == 0 else 1
+    piece_rows, piece_sources = chunk // pieces, span // pieces
+    split_last = fine == 2 and pieces == 2
     hidden_block = min(hidden, 256)
     column_block = min(full_width, 512)
     grad_block = min(full_width, 256)
@@ -72,6 +75,8 @@
     channels_pad = max(channels, 128)
     strip = full_width // n
     upright = strip % 128 == 0
+    halves = 2 if span == 2 and chips == 2 and groups == tp and upright else 1
+    half_width = width // halves
     levels = [1 << i for i in range((length - 1).bit_length())]
 
     def kernel(
@@ -80,7 +85,7 @@
         res_ref, proj_ref, conv_out, branch_out, gate_out, up_out, down_out,
         wg, wu, wd, key_t, gate_t, pick, send, full, hid, act, part, near, total, far, ret, rets,
         fullres_ref,
-        slopes, steps, decay, tails, speed, mix, gelu_val, gelu_slope, mix_grad, local,
+        slopes, steps, decay, tails, speed, mix_ref, gelu_val, gelu_slope, mix_grad, local,
         ends, ends_row, ends_all, carry, proj_part, proj_near, proj_sum, proj_far,
         es, er, xs, xr, zs, zr,
         ws, ss, sr, ys, yr, ps, pr, fs, fr, ns, nr, ts, tr, bs, br, gs, gr, hs, hr,
@@ -198,8 +203,8 @@
                 for i in range(begin, end):
                     dispatch_copy(j, i, 1).start()
 
-        def start_pass(j):
-            for i in range(fine):
+        def start_pass(j, begin=0, end=fine):
+            for i in range(begin, end):
                 u = j * fine + i
                 for t in range(1, chips):
                     block = full.at[unit_slice(j, i), :, :, columns(across(t, -1))]
@@ -208,8 +213,8 @@
                     ).wait_recv()
                     pass_on(j, i, t).start()
 
-        def end_pass(j):
-            for i in range(fine):
+        def end_pass(j, begin=0, end=fine):
+            for i in range(begin, end):
                 u = j * fine + i
                 block = full.at[unit_slice(j, i), :, :, columns(partner)]
                 remote(block, block, ps.at[u], pr.at[u], at(tp=partner)).wait_recv()
@@ -222,28 +227,36 @@
         def chunk_rows(j):
             return pl.ds(pl.multiple_of(group_of(j, -1) * chunk, 16), chunk)
 
-        def near_copy(j, t):
+        def near_copy(j, t, p=0, count=pieces):
+            base = group_of(j, -1) * chunk
+            rows = pl.ds(pl.multiple_of(base + p * piece_rows, 16), count * piece_rows)
             return remote(
-                part.at[chunk_rows(j), columns(turned(t, 1) * 2 + (1 - core))],
-                near.at[j, t], ns.at[j, t], nr.at[j, t], at(tp=partner),
+                part.at[rows, columns(turned(t, 1) * 2 + (1 - core))],
+                near.at[j, t, piece(p, count)], ns.at[j, t, p], nr.at[j, t, p], at(tp=partner),
             )
 
-        def far_copy(j, t):
+        def piece(p, count=1):
+            return pl.ds(pl.multiple_of(p * piece_rows, 16), count * piece_rows)
+
+        def far_copy(j, t, i):
             return remote(
-                total.at[j, t], far.at[j, t], ts.at[j, t], tr.at[j, t], at(tp=across(t, 1))
+                total.at[j, t, piece(i)], far.at[j, t, piece(i)],
+                ts.at[j, t, i], tr.at[j, t, i], at(tp=across(t, 1)),
             )
 
-        def compute(j):
-            base = group_of(j, -1) * span
-            where = chunk_rows(j)
+        def compute(j, p=0, count=pieces):
+            base = group_of(j, -1)
+            size = count * piece_rows
+            where = pl.ds(pl.multiple_of(base * chunk + p * piece_rows, 16), size)
+            sources = pl.ds(base * span + p * piece_sources, count * piece_sources)
 
             @pl.loop(0, hidden // hidden_block)
             def _(b):
                 cut = pl.ds(pl.multiple_of(b * hidden_block, hidden_block), hidden_block)
-                rows = full[pl.ds(base, span), 0].reshape(chunk, full_width)
+                rows = full[sources, 0].reshape(size, full_width)
                 pre_gate = jnp.dot(rows, wg[:, cut], preferred_element_type=f32)
                 pre_up = jnp.dot(rows, wu[:, cut], preferred_element_type=f32)
-                grads = full[pl.ds(base, span), 1].reshape(chunk, full_width)
+                grads = full[sources, 1].reshape(size, full_width)
                 act_grad = lax.dot_general(
                     grads, wd[cut, :], (((1,), (1,)), ((), ())), preferred_element_type=f32
                 )
@@ -254,47 +267,69 @@
                 hid[0, where, cut] = (act_grad * pre_up * slope).astype(bf16)
                 hid[1, where, cut] = (act_grad * silu).astype(bf16)
 
-            @pl.loop(0, full_width // column_block)
-            def _(b):
-                cut = pl.ds(pl.multiple_of(b * column_block, column_block), column_block)
-                value = lax.dot_general(
-                    hid[0, where, :], wg[cut, :], (((1,), (1,)), ((), ())), preferred_element_type=f32
-                ) + lax.dot_general(
-                    hid[1, where, :], wu[cut, :], (((1,), (1,)), ((), ())), preferred_element_type=f32
-                )
-                part[where, cut] = value.astype(bf16)
-
-            for t in range(chips):
-                near_copy(j, t).start()
+            @pl.loop(0, chips)
+            def _(turn):
+                t = lax.rem(turn + 1, chips)
+                for side in ((1 - core), core):
+                    cut = columns(turned(t, 1) * 2 + side)
+                    value = lax.dot_general(
+                        hid[0, where, :], wg[cut, :], (((1,), (1,)), ((), ())),
+                        preferred_element_type=f32,
+                    ) + lax.dot_general(
+                        hid[1, where, :], wu[cut, :], (((1,), (1,)), ((), ())),
+                        preferred_element_type=f32,
+                    )
+                    part[where, cut] = value.astype(bf16)
+                    if side is not core:
+                        near_copy(j, t, p, count).start()
+
+        def add_near(j, t, p):
+            where = pl.ds(pl.multiple_of(group_of(j, -1) * chunk + p * piece_rows, 16), piece_rows)
+            value = part[where, columns(turned(t, 1) * 2 + core)].astype(f32) + near[
+                j, t, piece(p)
+            ].astype(f32)
+            total[j, t, piece(p)] = value.astype(bf16)
+            far_copy(j, t, p).start()
 
         def reduce_near(j):
-            where = chunk_rows(j)
             for t in list(range(1, chips)) + [0]:
                 near_copy(j, t).wait_recv()
                 if t > 0:
-                    value = part[where, columns(turned(t, 1) * 2 + core)].astype(f32) + near[
-                        j, t
-                    ].astype(f32)
-                    total[j, t] = value.astype(bf16)
-                    far_copy(j, t).start()
-
-        def return_copy(j, i):
-            other = peer(j, i, -1)
-            k = j * span + i
-            return remote(ret.at[other], rets.at[me], bs.at[k], br.at[k], at(sp=other))
+                    for p in range(pieces):
+                        add_near(j, t, p)
+
+        def reduce_near_piece(j, p):
+            for t in list(range(1, chips)) + [0]:
+                near_copy(j, t, p, 1).wait_recv()
+                if t > 0:
+                    add_near(j, t, p)
+
+        def return_copy(j, source):
+            turn = lax.rem(inner - source + span, span)
+            k = j * span + turn
+            other = group_of(j, -1) * span + source
+            return k, remote(ret.at[other], rets.at[me], bs.at[k], br.at[k], at(sp=other))
+
+        def reduce_far_piece(j, p):
+            base = group_of(j, -1)
+            where = pl.ds(pl.multiple_of(base * chunk + p * piece_rows, 16), piece_rows)
+            value = part[where, mine].astype(f32) + near[j, 0, piece(p)].astype(f32)
+            for t in range(1, chips):
+                far_copy(j, t, p).wait_recv()
+                value = value + far[j, t, piece(p)].astype(f32)
+            ret[pl.ds(base * span + p * piece_sources, piece_sources)] = value.astype(
+                bf16
+            ).reshape(piece_sources, cap, width)
+            for s in range(piece_sources):
+                k, copy = return_copy(j, p * piece_sources + s)
+
+                @pl.when(k > 0)
+                def _():
+                    copy.start()
 
         def reduce_far(j):
-            where = chunk_rows(j)
-            value = part[where, mine].astype(f32) + near[j, 0].astype(f32)
-            for t in range(1, chips):
-                far_copy(j, t).wait_recv()
-                value = value + far[j, t].astype(f32)
-            ret[pl.ds(group_of(j, -1) * span, span)] = value.astype(bf16).reshape(span, cap, width)
-            for i in range(span):
-
-                @pl.when(j * span + i > 0)
-                def _():
-                    return_copy(j, i).start()
+            for p in range(pieces):
+                reduce_far_piece(j, p)
 
         if fine > 1:
             for copy in hand_over(0, 0):
@@ -377,14 +412,14 @@
             slope = half + 0.5 * value * (1.0 - tanh * tanh) * scale * (
                 1.0 + 3.0 * 0.044715 * value * value
             )
-            mix[rows, :] = (lru_out * gelu).astype(bf16)
+            mix_ref[rows, :] = (lru_out * gelu).astype(bf16)
             gelu_val[rows, :] = gelu
             gelu_slope[rows, :] = lru_out * slope
 
         for load in loads:
             load.wait()
 
-        @pl.loop(0, groups)
+        @pl.loop(0, groups - 1)
         def _(j):
             @pl.when(j < groups - 2)
             def _():
@@ -403,7 +438,7 @@
             def _():
                 start_forward(groups - 1, 1)
 
-            @pl.when((j > 0) & (j < groups - 1))
+            @pl.when(j > 0)
             def _():
                 reduce_near(j)
 
@@ -415,22 +450,53 @@
             def _():
                 reduce_far(j - 1)
 
-        reduce_near(groups - 1)
-        reduce_near(0)
+        final = groups - 1
+        if split_last:
+            early, late = lax.rem(inner + span, span), lax.rem(inner + span - 1, span)
+            start_pass(final, 0, 1)
+            end_pass(final, 0, 1)
+            compute(final, early, 1)
+            start_pass(final, 1)
+            reduce_near_piece(final, early)
+            end_pass(final, 1)
+            compute(final, late, 1)
+            reduce_near_piece(final, late)
+            reduce_near(0)
+            reduce_far(final - 1)
+            reduce_far_piece(final, early)
+        else:
+            late = pieces - 1
+            start_pass(final)
+            end_pass(final)
+            compute(final)
+            reduce_near(final)
+            reduce_near(0)
+            reduce_far(final - 1)
+            for p in range(pieces - 1):
+                reduce_far_piece(final, p)
         first_contract = (((0,), (0,)), ((), ()))
 
-        @pl.loop(0, full_width // grad_block)
-        def _(b):
-            cut = pl.ds(pl.multiple_of(b * grad_block, grad_block), grad_block)
-            rows = full[:, 0, :, cut].reshape(total_rows, grad_block)
-            gate_out[cut, :] = lax.dot_general(
-                rows, hid[0], first_contract, preferred_element_type=f32
-            ).astype(bf16)
-            up_out[cut, :] = lax.dot_general(
-                rows, hid[1], first_contract, preferred_element_type=f32
-            ).astype(bf16)
-
-        reduce_far(groups - 1)
+        grad_blocks = full_width // grad_block
+        middle = grad_blocks * 3 // 4
+        for begin, end in ((0, middle), (middle, grad_blocks)):
+            @pl.loop(begin, end)
+            def _(b):
+                cut = pl.ds(pl.multiple_of(b * grad_block, grad_block), grad_block)
+                rows = full[:, 0, :, cut].reshape(total_rows, grad_block)
+                gate_out[cut, :] = lax.dot_general(
+                    rows, hid[0], first_contract, preferred_element_type=f32
+                ).astype(bf16)
+                up_out[cut, :] = lax.dot_general(
+                    rows, hid[1], first_contract, preferred_element_type=f32
+                ).astype(bf16)
+
+            with jax.named_scope("S3"):
+                if begin == 0:
+                    reduce_far_piece(final, late)
+                else:
+                    reduce_far(0)
+                    rets[me] = ret[me]
+
         @pl.loop(0, full_width // grad_block)
         def _(b):
             cut = pl.ds(pl.multiple_of(b * grad_block, grad_block), grad_block)
@@ -439,9 +505,6 @@
                 act[...], grads, first_contract, preferred_element_type=f32
             ).astype(bf16)
 
-        reduce_far(0)
-        rets[me] = ret[me]
-
         @pl.loop(1, n)
         def _(k):
             j, i = k // span, k % span
@@ -456,26 +519,37 @@
         res_ref[...] = residual
         fullres_ref[:, mine] = residual
 
-        def gather_copy(t):
-            block = fullres_ref.at[:, mine]
+        def half_columns(member, h):
+            return pl.ds(pl.multiple_of(member * width + h * half_width, half_width), half_width)
+
+        def half_of(h):
+            return (1 - inner if h == 0 else inner) if halves == 2 else 0
+
+        def gather_copy(t, h):
+            block = fullres_ref.at[:, half_columns(place, half_of(h))]
             to = partner if t == 0 else across(t, 1)
-            return remote(block, block, gs.at[t], gr.at[t], at(tp=to))
-
-        def gather_pass(t):
-            block = fullres_ref.at[:, columns(across(t, -1))]
-            return remote(block, block, hs.at[t], hr.at[t], at(tp=partner))
-
-        for t in list(range(1, chips)) + [0]:
-            gather_copy(t).start()
-        for t in range(1, chips):
-            block = fullres_ref.at[:, columns(across(t, -1))]
-            remote(block, block, gs.at[t], gr.at[t], at(tp=across(t, -1))).wait_recv()
-            gather_pass(t).start()
-        block = fullres_ref.at[:, columns(partner)]
-        remote(block, block, gs.at[0], gr.at[0], at(tp=partner)).wait_recv()
-        for t in range(1, chips):
-            block = fullres_ref.at[:, columns(turned(t, -1) * 2 + (1 - core))]
-            remote(block, block, hs.at[t], hr.at[t], at(tp=partner)).wait_recv()
+            return remote(block, block, gs.at[t, h], gr.at[t, h], at(tp=to))
+
+        def gather_wait(t, h):
+            origin = partner if t == 0 else across(t, -1)
+            block = fullres_ref.at[:, half_columns(origin, half_of(h))]
+            return remote(block, block, gs.at[t, h], gr.at[t, h], at(tp=origin))
+
+        def gather_pass(t, h):
+            block = fullres_ref.at[:, half_columns(across(t, -1), half_of(h))]
+            return remote(block, block, hs.at[t, h], hr.at[t, h], at(tp=partner))
+
+        def pass_wait(t, h):
+            block = fullres_ref.at[
+                :, half_columns(turned(t, -1) * 2 + (1 - core), half_of(h))
+            ]
+            return remote(block, block, hs.at[t, h], hr.at[t, h], at(tp=partner))
+
+        for h in range(halves):
+            for t in range(1, chips):
+                gather_copy(t, h).start()
+        for h in range(halves):
+            gather_copy(0, h).start()
 
         def strip_of(g, i):
             other = g * span + i
@@ -514,15 +588,23 @@
             where = pl.ds(pl.multiple_of(outer_peer(g, 1) * turn_width, turn_width), turn_width)
             if upright:
                 proj_part[:, where] = jnp.dot(
-                    mix[...], fullres_ref[:, where], preferred_element_type=f32
+                    mix_ref[...], fullres_ref[:, where], preferred_element_type=f32
                 ).astype(bf16)
             else:
                 proj_part[where, :] = lax.dot_general(
-                    fullres_ref[:, where], mix[...], (((0,), (1,)), ((), ())),
+                    fullres_ref[:, where], mix_ref[...], (((0,), (1,)), ((), ())),
                     preferred_element_type=f32,
                 ).astype(bf16)
             for i in range(1, span):
                 inner_copy(g, i).start()
+
+        def project_half(member, h):
+            where = half_columns(member, half_of(h))
+            proj_part[:, where] = jnp.dot(
+                mix_ref[...], fullres_ref[:, where], preferred_element_type=f32
+            ).astype(bf16)
+            if h == 0:
+                inner_copy(lax.rem(member - group + groups, groups), 1).start()
 
         def finish_inner(g):
             total_strip = read_strip(outer_peer(g, 1) * span + inner)
@@ -530,10 +612,39 @@
                 inner_copy(g, i).wait_recv()
                 total_strip = total_strip + proj_near[g, i].astype(f32)
             proj_sum[g] = total_strip.astype(bf16)
-            if g > 0:
+
+            @pl.when(g > 0)
+            def _():
                 outer_copy(g).start()
 
-        project(turns[0])
+        other_side = turned(1, -1) * 2
+        if halves == 2:
+            project_half(place, 0)
+            gather_wait(1, 0).wait_recv()
+            gather_pass(1, 0).start()
+            project_half(other_side + core, 0)
+            pass_wait(1, 0).wait_recv()
+            project_half(other_side + (1 - core), 0)
+            gather_wait(0, 0).wait_recv()
+            project_half(partner, 0)
+            project_half(place, 1)
+            finish_inner(lax.rem(place - group + groups, groups))
+            gather_wait(1, 1).wait_recv()
+            gather_pass(1, 1).start()
+            gather_wait(0, 1).wait_recv()
+            project_half(partner, 1)
+            project_half(other_side + core, 1)
+            pass_wait(1, 1).wait_recv()
+            project_half(other_side + (1 - core), 1)
+        else:
+            for t in range(1, chips):
+                gather_wait(t, 0).wait_recv()
+                gather_pass(t, 0).start()
+            gather_wait(0, 0).wait_recv()
+            for t in range(1, chips):
+                pass_wait(t, 0).wait_recv()
+            for g in turns[:2]:
+                project(g)
         mix_grad[...] = lax.dot_general(
             outp_ref[...], fullres_ref[...], (((1,), (1,)), ((), ())), preferred_element_type=f32
         )
@@ -571,10 +682,15 @@
 
         ends_all[me] = ends_row[...]
 
-        for g in turns[1:]:
-            project(g)
-        for g in turns[:-2]:
-            finish_inner(g)
+        if halves == 2:
+            finish_inner(lax.rem(other_side + core - group + groups, groups))
+            finish_inner(lax.rem(other_side + (1 - core) - group + groups, groups))
+            finish_inner(lax.rem(partner - group + groups, groups))
+        else:
+            for g in turns[2:]:
+                project(g)
+            for g in turns[:-2]:
+                finish_inner(g)
         @pl.loop(1, n)
         def _(k):
             origin = lax.rem(me - k + n, n)
@@ -611,8 +727,9 @@
                 )
             conv_out[rows, :] = value
 
-        for g in turns[-2:]:
-            finish_inner(g)
+        if halves == 1:
+            for g in turns[-2:]:
+                finish_inner(g)
         summed = proj_sum[0].astype(f32)
         for g in turns[:-1]:
             outer_copy(g).wait_recv()
@@ -633,7 +750,8 @@
         def _(k):
             j, i = k // span, k % span
             dispatch_copy(j, i, 1).wait_send()
-            return_copy(j, i).wait_send()
+            source = peer(j, i, -1)
+            remote(ret.at[source], rets.at[me], bs.at[k], br.at[k], at(sp=source)).wait_send()
 
         @pl.loop(0, groups)
         def _(j):
@@ -643,14 +761,26 @@
                 for t in range(1, chips):
                     pass_on(j, i, t).wait_send()
             for t in range(chips):
-                near_copy(j, t).wait_send()
+                if split_last:
+                    for p in range(pieces):
+                        @pl.when(j == groups - 1)
+                        def _():
+                            near_copy(j, t, p, 1).wait_send()
+
+                    @pl.when(j < groups - 1)
+                    def _():
+                        near_copy(j, t).wait_send()
+                else:
+                    near_copy(j, t).wait_send()
             for t in range(1, chips):
-                far_copy(j, t).wait_send()
-
-        for t in range(chips):
-            gather_copy(t).wait_send()
-        for t in range(1, chips):
-            gather_pass(t).wait_send()
+                for p in range(pieces):
+                    far_copy(j, t, p).wait_send()
+
+        for h in range(halves):
+            for t in range(chips):
+                gather_copy(t, h).wait_send()
+            for t in range(1, chips):
+                gather_pass(t, h).wait_send()
 
 
     dma = pltpu.SemaphoreType.DMA
@@ -699,7 +829,7 @@
         + sem(n) + sem(groups, span) + sem(groups)
         + [dma((3,))]
         + sem(n) + sem(units, wide) + sem(units) + sem(units, wide)
-        + sem(groups, wide) + sem(groups, wide) + sem(n) + sem(wide) + sem(wide),
+        + sem(groups, wide, pieces) + sem(groups, wide, pieces) + sem(n) + sem(wide, halves) + sem(wide, halves),
         compiler_params=pltpu.CompilerParams(
             collective_id=1, has_side_effects=True, vmem_limit_bytes=54 * 1024 * 1024
         ),

time: 105 us -> 99.7 us (0.950)
  Pallas kernels: 103 us -> 98.2 us
    pallas_call x1, Pallas kernels: 99.7 us -> 95.1 us  [layer_backward(): pl.pallas_call(kernel, name='layer_backward', out_shape=(pltpu.VMEM((toke...]
where the time goes in v3:
time: 99.7 us; the launch traced here: 98.9 us
  Pallas kernels  98.2 us (98%)
    pallas_call x1, Pallas kernels, layer_backward(): pl.pallas_call(kernel, name='layer_backward', out_shape=(pltpu.VMEM((toke...  95.1 us
    pallas_call x1, Pallas kernels, write_out(): pl.pallas_call(kernel, name='write_out', out_shape=tuple((jax.ShapeDtypeS...  3.11 us

profile of v3, /device:TPU:5, one launch (start us, length us, event | category | flops | bytes accessed | tf_op | source)
XLA Modules:
  0.0 98.9 jit_solution(13314158480322851443)
XLA Ops:
  0.6 95.1 %layer_backward.1 = (bf16[256,512]{1,0:T(8,128)(2,1)S(1)}, f32[256,256]{1,0:T(8,128)S(1)}, f32[256,256]{1,0:T(8,128)S(1)}, f32[256,256]{1,0:T(8,128)S(1)}, bf16[...) custom-call(bf16[256,512]{1,0:T(8,128)(2,1)} %cot_ref.1, ...), custom_call_target="tpu_custom_call" | custom-call | tf_op jit(solution)/shard_map/layer_backward/pallas_call | solution.py:793
  95.8 3.1 %write_out.1 = (bf16[256,512]{1,0:T(8,128)(2,1)}, f32[256,256]{1,0:T(8,128)}, f32[256,256]{1,0:T(8,128)}, f32[256,256]{1,0:T(8,128)}, bf16[2048,512]{1,0:T(8,128...) custom-call(bf16[256,512]{1,0:T(8,128)(2,1)S(1)} %get-tuple-element.21.refs_0_, ...), custom_call_target="tpu_custom_call" | custom-call | tf_op jit(solution)/shard_map/write_out/pallas_call | solution.py:855

commit v4 on v3

--- a/solution.py
+++ b/solution.py
@@ -18,11 +18,14 @@
     return (sp, tp)
 
 
-def meet(devices):
+def greet(devices):
     barrier = pltpu.get_barrier_semaphore()
     for device in devices:
         pl.semaphore_signal(barrier, inc=1, device_id=device, device_id_type=MESH)
-    pl.semaphore_wait(barrier, len(devices))
+
+
+def await_greetings(count):
+    pl.semaphore_wait(pltpu.get_barrier_semaphore(), count)
 
 
 def remote(source, target, send, recv, device):
@@ -77,13 +80,16 @@
     upright = strip % 128 == 0
     halves = 2 if span == 2 and chips == 2 and groups == tp and upright else 1
     half_width = width // halves
+    quarters = 2 if halves == 2 and strip % 256 == 0 else 1
+    quarter_width, slice_width = half_width // quarters, strip // quarters
+    scan_rows = min(channels, 128)
     levels = [1 << i for i in range((length - 1).bit_length())]
 
     def kernel(
         cot_ref, in_ref, routes_ref, gates_ref, conv_ref, branch_ref, before_ref, after_ref,
         jump_ref, wr_ref, wi_ref, lam_ref, outp_ref, wg_hbm, wu_hbm, wd_hbm,
         res_ref, proj_ref, conv_out, branch_out, gate_out, up_out, down_out,
-        wg, wu, wd, key_t, gate_t, pick, send, full, hid, act, part, near, total, far, ret, rets,
+        wg, wu, wd, wg_t, wu_t, wd_t, key_t, gate_t, pick, send, full, hid, act, part, near, total, far, ret, rets,
         fullres_ref,
         slopes, steps, decay, tails, speed, mix_ref, gelu_val, gelu_slope, mix_grad, local,
         ends, ends_row, ends_all, carry, proj_part, proj_near, proj_sum, proj_far,
@@ -120,7 +126,7 @@
         for load in loads:
             load.start()
 
-        meet(
+        greet(
             [at(sp=lax.rem(me + k, n)) for k in range(1, n)]
             + [at(tp=partner)]
             + [at(tp=across(t, 1)) for t in range(1, chips)]
@@ -257,9 +263,7 @@
                 pre_gate = jnp.dot(rows, wg[:, cut], preferred_element_type=f32)
                 pre_up = jnp.dot(rows, wu[:, cut], preferred_element_type=f32)
                 grads = full[sources, 1].reshape(size, full_width)
-                act_grad = lax.dot_general(
-                    grads, wd[cut, :], (((1,), (1,)), ((), ())), preferred_element_type=f32
-                )
+                act_grad = jnp.dot(grads, wd_t[:, cut], preferred_element_type=f32)
                 sigmoid = jax.nn.sigmoid(pre_gate)
                 silu = pre_gate * sigmoid
                 slope = sigmoid * (1.0 + pre_gate * (1.0 - sigmoid))
@@ -272,13 +276,9 @@
                 t = lax.rem(turn + 1, chips)
                 for side in ((1 - core), core):
                     cut = columns(turned(t, 1) * 2 + side)
-                    value = lax.dot_general(
-                        hid[0, where, :], wg[cut, :], (((1,), (1,)), ((), ())),
-                        preferred_element_type=f32,
-                    ) + lax.dot_general(
-                        hid[1, where, :], wu[cut, :], (((1,), (1,)), ((), ())),
-                        preferred_element_type=f32,
-                    )
+                    value = jnp.dot(
+                        hid[0, where, :], wg_t[:, cut], preferred_element_type=f32
+                    ) + jnp.dot(hid[1, where, :], wu_t[:, cut], preferred_element_type=f32)
                     part[where, cut] = value.astype(bf16)
                     if side is not core:
                         near_copy(j, t, p, count).start()
@@ -331,21 +331,31 @@
             for p in range(pieces):
                 reduce_far_piece(j, p)
 
+        @pl.loop(1, n)
+        def _(k):
+            to = peer(k // span, k % span, 1)
+            rows, grads = packed(to)
+            send[to, 0] = rows
+            send[to, 1] = grads
+
+        await_greetings(n + chips - 1)
         if fine > 1:
             for copy in hand_over(0, 0):
                 copy.start()
 
-        @pl.loop(1, n)
+        @pl.loop(1, 2 * span)
         def _(k):
-            j, i = k // span, k % span
-            to = peer(j, i, 1)
-            rows, grads = packed(to)
-            send[to, 0] = rows
-            send[to, 1] = grads
-
-            @pl.when(j < 2)
-            def _():
-                dispatch_copy(j, i, 1).start()
+            dispatch_copy(k // span, k % span, 1).start()
+
+        for load in loads:
+            load.wait()
+
+        @pl.loop(0, full_width // grad_block)
+        def _(b):
+            cut = pl.ds(pl.multiple_of(b * grad_block, grad_block), grad_block)
+            wd_t[cut, :] = wd[:, cut].T
+            wg_t[:, cut] = wg[cut, :].T
+            wu_t[:, cut] = wu[cut, :].T
 
         start_forward(0, 1 if fine > 1 else 0)
         release(2, 0, span)
@@ -358,12 +368,12 @@
                 jnp.where(diagonal, lam_ref[d : d + 1, :], 0.0), axis=1, keepdims=True
             )
             speed[d] = decay_scale * softplus(-jnp.broadcast_to(column, (channels, 128)))
-        token = lax.broadcasted_iota(jnp.int32, (block_width, length), 1)
 
         def shifted(value, by, d):
             return pltpu.roll(value, length - by if d == 0 else by, 1)
 
-        def inside(by, d):
+        def inside(by, d, rows=block_width):
+            token = lax.broadcasted_iota(jnp.int32, (rows, length), 1)
             return token < length - by if d == 0 else token >= by
 
         @pl.loop(0, blocks)
@@ -416,8 +426,6 @@
             gelu_val[rows, :] = gelu
             gelu_slope[rows, :] = lru_out * slope
 
-        for load in loads:
-            load.wait()
 
         @pl.loop(0, groups - 1)
         def _(j):
@@ -519,47 +527,50 @@
         res_ref[...] = residual
         fullres_ref[:, mine] = residual
 
-        def half_columns(member, h):
-            return pl.ds(pl.multiple_of(member * width + h * half_width, half_width), half_width)
+        def half_columns(member, h, q):
+            start = member * width + h * half_width + q * quarter_width
+            return pl.ds(pl.multiple_of(start, quarter_width), quarter_width)
 
         def half_of(h):
             return (1 - inner if h == 0 else inner) if halves == 2 else 0
 
-        def gather_copy(t, h):
-            block = fullres_ref.at[:, half_columns(place, half_of(h))]
+        parts = [(h, q) for q in range(quarters) for h in range(halves)]
+
+        def gather_copy(t, h, q):
+            block = fullres_ref.at[:, half_columns(place, half_of(h), q)]
             to = partner if t == 0 else across(t, 1)
-            return remote(block, block, gs.at[t, h], gr.at[t, h], at(tp=to))
-
-        def gather_wait(t, h):
+            return remote(block, block, gs.at[t, h, q], gr.at[t, h, q], at(tp=to))
+
+        def gather_wait(t, h, q):
             origin = partner if t == 0 else across(t, -1)
-            block = fullres_ref.at[:, half_columns(origin, half_of(h))]
-            return remote(block, block, gs.at[t, h], gr.at[t, h], at(tp=origin))
-
-        def gather_pass(t, h):
-            block = fullres_ref.at[:, half_columns(across(t, -1), half_of(h))]
-            return remote(block, block, hs.at[t, h], hr.at[t, h], at(tp=partner))
-
-        def pass_wait(t, h):
+            block = fullres_ref.at[:, half_columns(origin, half_of(h), q)]
+            remote(block, block, gs.at[t, h, q], gr.at[t, h, q], at(tp=origin)).wait_recv()
+
+        def gather_pass(t, h, q):
+            block = fullres_ref.at[:, half_columns(across(t, -1), half_of(h), q)]
+            return remote(block, block, hs.at[t, h, q], hr.at[t, h, q], at(tp=partner))
+
+        def pass_wait(t, h, q):
             block = fullres_ref.at[
-                :, half_columns(turned(t, -1) * 2 + (1 - core), half_of(h))
+                :, half_columns(turned(t, -1) * 2 + (1 - core), half_of(h), q)
             ]
-            return remote(block, block, hs.at[t, h], hr.at[t, h], at(tp=partner))
-
-        for h in range(halves):
+            remote(block, block, hs.at[t, h, q], hr.at[t, h, q], at(tp=partner)).wait_recv()
+
+        for h, q in parts:
             for t in range(1, chips):
-                gather_copy(t, h).start()
-        for h in range(halves):
-            gather_copy(0, h).start()
-
-        def strip_of(g, i):
-            other = g * span + i
+                gather_copy(t, h, q).start()
+        for h, q in parts:
+            gather_copy(0, h, q).start()
+
+        def strip_at(other, q):
+            start = pl.multiple_of(other * strip + q * slice_width, slice_width)
             if upright:
-                return proj_part.at[:, pl.ds(pl.multiple_of(other * strip, strip), strip)]
-            return proj_part.at[pl.ds(pl.multiple_of(other * strip, strip), strip), :]
-
-        def read_strip(other):
-            where = pl.ds(pl.multiple_of(other * strip, strip), strip)
-            return (proj_part[:, where] if upright else proj_part[where, :]).astype(f32)
+                return (slice(None), pl.ds(start, slice_width))
+            return (pl.ds(start, slice_width), slice(None))
+
+        def slice_at(q):
+            cut = pl.ds(q * slice_width, slice_width)
+            return (slice(None), cut) if upright else (cut, slice(None))
 
         def inner_peer(i, sign):
             return lax.rem(inner + sign * i + span, span)
@@ -567,17 +578,17 @@
         def outer_peer(g, sign):
             return lax.rem(group + sign * g + groups, groups)
 
-        def inner_copy(g, i):
-            other = outer_peer(g, 1)
+        def inner_copy(g, i, q=0):
+            other = outer_peer(g, 1) * span + inner_peer(i, 1)
             return remote(
-                strip_of(other, inner_peer(i, 1)), proj_near.at[g, i], xs.at[g, i], xr.at[g, i],
-                at(sp=group * span + inner_peer(i, 1)),
-            )
-
-        def outer_copy(g):
+                proj_part.at[strip_at(other, q)], proj_near.at[(g, i) + slice_at(q)],
+                xs.at[g, i, q], xr.at[g, i, q], at(sp=group * span + inner_peer(i, 1)),
+            )
+
+        def outer_copy(g, q=0):
             return remote(
-                proj_sum.at[g], proj_far.at[g], zs.at[g], zr.at[g],
-                at(sp=outer_peer(g, 1) * span + inner),
+                proj_sum.at[(g,) + slice_at(q)], proj_far.at[(g,) + slice_at(q)],
+                zs.at[g, q], zr.at[g, q], at(sp=outer_peer(g, 1) * span + inner),
             )
 
         turns = list(range(1, groups))
@@ -598,61 +609,87 @@
             for i in range(1, span):
                 inner_copy(g, i).start()
 
-        def project_half(member, h):
-            where = half_columns(member, half_of(h))
+        def turn_to(member):
+            return lax.rem(member - group + groups, groups)
+
+        def project_piece(member, h, q):
+            where = half_columns(member, half_of(h), q)
             proj_part[:, where] = jnp.dot(
                 mix_ref[...], fullres_ref[:, where], preferred_element_type=f32
             ).astype(bf16)
             if h == 0:
-                inner_copy(lax.rem(member - group + groups, groups), 1).start()
-
-        def finish_inner(g):
-            total_strip = read_strip(outer_peer(g, 1) * span + inner)
+                inner_copy(turn_to(member), 1, q).start()
+
+        def add_mix_grad(member, begin=False):
+            where = columns(member)
+            value = lax.dot_general(
+                outp_ref[:, where], fullres_ref[:, where], (((1,), (1,)), ((), ())),
+                preferred_element_type=f32,
+            )
+            mix_grad[...] = value if begin else mix_grad[...] + value
+
+        def finish_inner(g, q=0):
+            total_strip = proj_part[strip_at(outer_peer(g, 1) * span + inner, q)].astype(f32)
             for i in range(1, span):
-                inner_copy(g, i).wait_recv()
-                total_strip = total_strip + proj_near[g, i].astype(f32)
-            proj_sum[g] = total_strip.astype(bf16)
+                inner_copy(g, i, q).wait_recv()
+                total_strip = total_strip + proj_near[(g, i) + slice_at(q)].astype(f32)
+            proj_sum[(g,) + slice_at(q)] = total_strip.astype(bf16)
 
             @pl.when(g > 0)
             def _():
-                outer_copy(g).start()
-
-        other_side = turned(1, -1) * 2
+                outer_copy(g, q).start()
+
+        far_side = turned(1, -1) * 2 + core
+        far_pair = turned(1, -1) * 2 + (1 - core)
         if halves == 2:
-            project_half(place, 0)
-            gather_wait(1, 0).wait_recv()
-            gather_pass(1, 0).start()
-            project_half(other_side + core, 0)
-            pass_wait(1, 0).wait_recv()
-            project_half(other_side + (1 - core), 0)
-            gather_wait(0, 0).wait_recv()
-            project_half(partner, 0)
-            project_half(place, 1)
-            finish_inner(lax.rem(place - group + groups, groups))
-            gather_wait(1, 1).wait_recv()
-            gather_pass(1, 1).start()
-            gather_wait(0, 1).wait_recv()
-            project_half(partner, 1)
-            project_half(other_side + core, 1)
-            pass_wait(1, 1).wait_recv()
-            project_half(other_side + (1 - core), 1)
+            for q in range(quarters):
+                for h in range(halves):
+                    project_piece(place, h, q)
+            add_mix_grad(place, True)
+            for h, q in parts:
+                gather_wait(0, h, q)
+            for h in range(halves):
+                project_piece(partner, h, 0)
+            for q in range(quarters):
+                for h in range(halves):
+                    gather_wait(1, h, q)
+                    gather_pass(1, h, q).start()
+                    project_piece(far_side, h, q)
+                    if q == 0 and h == 0:
+                        add_mix_grad(partner)
+                if q == 0:
+                    for done in range(quarters):
+                        finish_inner(turn_to(place), done)
+                else:
+                    finish_inner(turn_to(far_side), 0)
+                    add_mix_grad(far_side)
+                for h in range(halves):
+                    pass_wait(1, h, q)
+                    project_piece(far_pair, h, q)
+                if q == 0:
+                    for h in range(halves):
+                        project_piece(partner, h, 1)
+                    finish_inner(turn_to(partner), 0)
+            add_mix_grad(far_pair)
         else:
             for t in range(1, chips):
-                gather_wait(t, 0).wait_recv()
-                gather_pass(t, 0).start()
-            gather_wait(0, 0).wait_recv()
+                gather_wait(t, 0, 0)
+                gather_pass(t, 0, 0).start()
+            gather_wait(0, 0, 0)
             for t in range(1, chips):
-                pass_wait(t, 0).wait_recv()
+                pass_wait(t, 0, 0)
             for g in turns[:2]:
                 project(g)
-        mix_grad[...] = lax.dot_general(
-            outp_ref[...], fullres_ref[...], (((1,), (1,)), ((), ())), preferred_element_type=f32
-        )
-        lane = lax.broadcasted_iota(jnp.int32, (block_width, 128), 1)
-
-        @pl.loop(0, blocks)
+        if halves == 1:
+            mix_grad[...] = lax.dot_general(
+                outp_ref[...], fullres_ref[...], (((1,), (1,)), ((), ())),
+                preferred_element_type=f32,
+            )
+        lane = lax.broadcasted_iota(jnp.int32, (scan_rows, 128), 1)
+
+        @pl.loop(0, channels // scan_rows)
         def _(b):
-            rows = pl.ds(pl.multiple_of(b * block_width, block_width), block_width)
+            rows = pl.ds(pl.multiple_of(b * scan_rows, scan_rows), scan_rows)
             upper = mix_grad[rows, :]
             branch_out[rows, :] = upper * gelu_slope[rows, :]
             grad = upper * gelu_val[rows, :]
@@ -661,7 +698,7 @@
                 carried = decay[d, rows, :] * grad
                 for level, by in enumerate(levels):
                     carried = carried + steps[d, level, rows, :] * shifted(carried, by, d)
-                local[d, rows, :] = grad + jnp.where(inside(1, d), shifted(carried, 1, d), 0.0)
+                local[d, rows, :] = grad + jnp.where(inside(1, d, scan_rows), shifted(carried, 1, d), 0.0)
                 last.append(carried[:, 0:1] if d == 0 else carried[:, length - 1 : length])
             packed_ends = jnp.where(lane == 0, last[0], jnp.where(lane == 1, last[1], 0.0))
             packed_ends = jnp.where(lane == 2, slopes[0, 3, rows, 0:128], packed_ends)
@@ -683,9 +720,10 @@
         ends_all[me] = ends_row[...]
 
         if halves == 2:
-            finish_inner(lax.rem(other_side + core - group + groups, groups))
-            finish_inner(lax.rem(other_side + (1 - core) - group + groups, groups))
-            finish_inner(lax.rem(partner - group + groups, groups))
+            finish_inner(turn_to(far_pair), 0)
+            finish_inner(turn_to(partner), 1)
+            finish_inner(turn_to(far_side), 1)
+            finish_inner(turn_to(far_pair), 1)
         else:
             for g in turns[2:]:
                 project(g)
@@ -732,15 +770,17 @@
                 finish_inner(g)
         summed = proj_sum[0].astype(f32)
         for g in turns[:-1]:
-            outer_copy(g).wait_recv()
+            for q in range(quarters):
+                outer_copy(g, q).wait_recv()
             summed = summed + proj_far[g].astype(f32)
         proj_ref[...] = summed if upright else summed.T
 
         for g in turns:
-            for i in range(1, span):
-                inner_copy(g, i).wait_send()
-            if g > 0:
-                outer_copy(g).wait_send()
+            for q in range(quarters):
+                for i in range(1, span):
+                    inner_copy(g, i, q).wait_send()
+                if g > 0:
+                    outer_copy(g, q).wait_send()
 
         @pl.loop(1, n)
         def _(k):
@@ -776,11 +816,11 @@
                 for p in range(pieces):
                     far_copy(j, t, p).wait_send()
 
-        for h in range(halves):
+        for h, q in parts:
             for t in range(chips):
-                gather_copy(t, h).wait_send()
+                gather_copy(t, h, q).wait_send()
             for t in range(1, chips):
-                gather_pass(t, h).wait_send()
+                gather_pass(t, h, q).wait_send()
 
 
     dma = pltpu.SemaphoreType.DMA
@@ -801,6 +841,8 @@
         out_specs=(VMEM_SPEC,) * 7,
         scratch_shapes=[
             pltpu.VMEM(w_gate.shape, bf16), pltpu.VMEM(w_up.shape, bf16), pltpu.VMEM(w_down.shape, bf16),
+            pltpu.VMEM((hidden, full_width), bf16), pltpu.VMEM((hidden, full_width), bf16),
+            pltpu.VMEM((full_width, hidden), bf16),
             pltpu.VMEM((128, tokens), f32), pltpu.VMEM((128, tokens), f32),
             pltpu.VMEM((total_rows, tokens), bf16),
             pltpu.VMEM((n, 2, cap, width), bf16),
@@ -826,10 +868,10 @@
             pltpu.VMEM((groups, span) + strip_shape, bf16),
             pltpu.VMEM((groups,) + strip_shape, bf16), pltpu.VMEM((groups,) + strip_shape, bf16),
         ]
-        + sem(n) + sem(groups, span) + sem(groups)
+        + sem(n) + sem(groups, span, quarters) + sem(groups, quarters)
         + [dma((3,))]
         + sem(n) + sem(units, wide) + sem(units) + sem(units, wide)
-        + sem(groups, wide, pieces) + sem(groups, wide, pieces) + sem(n) + sem(wide, halves) + sem(wide, halves),
+        + sem(groups, wide, pieces) + sem(groups, wide, pieces) + sem(n) + sem(wide, halves, quarters) + sem(wide, halves, quarters),
         compiler_params=pltpu.CompilerParams(
             collective_id=1, has_side_effects=True, vmem_limit_bytes=54 * 1024 * 1024
         ),

time: 99.7 us -> 95.3 us (0.956)
  Pallas kernels: 98.2 us -> 94.5 us
    pallas_call x1, Pallas kernels: 95.1 us -> 91.4 us  [layer_backward(): pl.pallas_call(kernel, name='layer_backward', out_shape=(pltpu.VMEM((toke...]
where the time goes in v4:
time: 95.3 us; the launch traced here: 95.1 us
  Pallas kernels  94.5 us (99%)
    pallas_call x1, Pallas kernels, layer_backward(): pl.pallas_call(kernel, name='layer_backward', out_shape=(pltpu.VMEM((toke...  91.4 us
    pallas_call x1, Pallas kernels, write_out(): pl.pallas_call(kernel, name='write_out', out_shape=tuple((jax.ShapeDtypeS...  3.11 us

profile of v4, /device:TPU:5, one launch (start us, length us, event | category | flops | bytes accessed | tf_op | source)
XLA Modules:
  0.0 95.1 jit_solution(17820002613212767776)
XLA Ops:
  0.6 91.4 %layer_backward.1 = (bf16[256,512]{1,0:T(8,128)(2,1)S(1)}, f32[256,256]{1,0:T(8,128)S(1)}, f32[256,256]{1,0:T(8,128)S(1)}, f32[256,256]{1,0:T(8,128)S(1)}, bf16[...) custom-call(bf16[256,512]{1,0:T(8,128)(2,1)} %cot_ref.1, ...), custom_call_target="tpu_custom_call" | custom-call | tf_op jit(solution)/shard_map/layer_backward/pallas_call | solution.py:833
  92.0 3.1 %write_out.1 = (bf16[256,512]{1,0:T(8,128)(2,1)}, f32[256,256]{1,0:T(8,128)}, f32[256,256]{1,0:T(8,128)}, f32[256,256]{1,0:T(8,128)}, bf16[2048,512]{1,0:T(8,128...) custom-call(bf16[256,512]{1,0:T(8,128)(2,1)S(1)} %get-tuple-element.21.refs_0_, ...), custom_call_target="tpu_custom_call" | custom-call | tf_op jit(solution)/shard_map/write_out/pallas_call | solution.py:897

commit v5 on v4

--- a/solution.py
+++ b/solution.py
@@ -343,7 +343,7 @@
             for copy in hand_over(0, 0):
                 copy.start()
 
-        @pl.loop(1, 2 * span)
+        @pl.loop(1, span + half)
         def _(k):
             dispatch_copy(k // span, k % span, 1).start()
 
@@ -357,6 +357,7 @@
             wg_t[:, cut] = wg[cut, :].T
             wu_t[:, cut] = wu[cut, :].T
 
+        release(1, half, span)
         start_forward(0, 1 if fine > 1 else 0)
         release(2, 0, span)
 
@@ -648,8 +649,6 @@
             add_mix_grad(place, True)
             for h, q in parts:
                 gather_wait(0, h, q)
-            for h in range(halves):
-                project_piece(partner, h, 0)
             for q in range(quarters):
                 for h in range(halves):
                     gather_wait(1, h, q)
@@ -667,9 +666,9 @@
                     pass_wait(1, h, q)
                     project_piece(far_pair, h, q)
                 if q == 0:
-                    for h in range(halves):
-                        project_piece(partner, h, 1)
-                    finish_inner(turn_to(partner), 0)
+                    for r in range(quarters):
+                        for h in range(halves):
+                            project_piece(partner, h, r)
             add_mix_grad(far_pair)
         else:
             for t in range(1, chips):
@@ -721,6 +720,7 @@
 
         if halves == 2:
             finish_inner(turn_to(far_pair), 0)
+            finish_inner(turn_to(partner), 0)
             finish_inner(turn_to(partner), 1)
             finish_inner(turn_to(far_side), 1)
             finish_inner(turn_to(far_pair), 1)

time: 95.3 us -> 95.1 us (level)
  no operation moved by 1% of the time
where the time goes in v5:
time: 95.1 us; the launch traced here: 94.9 us
  Pallas kernels  94.3 us (99%)
    pallas_call x1, Pallas kernels, layer_backward(): pl.pallas_call(kernel, name='layer_backward', out_shape=(pltpu.VMEM((toke...  91.1 us
    pallas_call x1, Pallas kernels, write_out(): pl.pallas_call(kernel, name='write_out', out_shape=tuple((jax.ShapeDtypeS...  3.11 us

profile of v5, /device:TPU:5, one launch (start us, length us, event | category | flops | bytes accessed | tf_op | source)
XLA Modules:
  0.0 94.9 jit_solution(18175822023398666671)
XLA Ops:
  0.6 91.1 %layer_backward.1 = (bf16[256,512]{1,0:T(8,128)(2,1)S(1)}, f32[256,256]{1,0:T(8,128)S(1)}, f32[256,256]{1,0:T(8,128)S(1)}, f32[256,256]{1,0:T(8,128)S(1)}, bf16[...) custom-call(bf16[256,512]{1,0:T(8,128)(2,1)} %cot_ref.1, ...), custom_call_target="tpu_custom_call" | custom-call | tf_op jit(solution)/shard_map/layer_backward/pallas_call | solution.py:833
  91.8 3.1 %write_out.1 = (bf16[256,512]{1,0:T(8,128)(2,1)}, f32[256,256]{1,0:T(8,128)}, f32[256,256]{1,0:T(8,128)}, f32[256,256]{1,0:T(8,128)}, bf16[2048,512]{1,0:T(8,128...) custom-call(bf16[256,512]{1,0:T(8,128)(2,1)S(1)} %get-tuple-element.21.refs_0_, ...), custom_call_target="tpu_custom_call" | custom-call | tf_op jit(solution)/shard_map/write_out/pallas_call | solution.py:897
